TPU v7x, 32 devices: a whole 2x2x4 slice. The times are simulated.
32 devices in a mesh: ep: 8 (over z, y), tp: 4 (over x, core).
Axes of the slice: x: 2, y: 2, z: 4, core: 2. Of those that a mesh axis runs over, the one named last changes fastest.
Arguments:
- queries: bfloat16 [4096, 2048], P('ep', 'tp'), may hold values from -6 to 6
- key_rows: bfloat16 [4096, 2048], P('ep', 'tp'), may hold values from -6 to 6
- value_rows: bfloat16 [4096, 4096], P('ep', 'tp'), may hold values from -6 to 6
- gate_rows: bfloat16 [4096, 4096], P('ep', 'tp'), may hold values from -6 to 6
- log_decay: float32 [16, 4096], P('tp', 'ep'), may hold values from -1 to 0
- head_gain: float32 [4096], P('tp'), may hold values from 0.1 to 1.9
- out_weight: bfloat16 [4096, 4096], P('tp'), may hold values from -0.09375 to 0.09375
- expert_input: bfloat16 [4096, 4096], P('ep'), may hold values from -6 to 6
- input_gain: float32 [4096], replicated, may hold values from 0.1 to 1.9
- route_ids: int32 [4096, 2], P('ep'), may hold values from 0 to 7, as said below
- route_weight: float32 [4096, 2], P('ep'), may hold values from 0.1 to 0.9
- expert_gate: bfloat16 [8, 4096, 1024], P('ep', None, 'tp'), may hold values from -0.09375 to 0.09375
- expert_up: bfloat16 [8, 4096, 1024], P('ep', None, 'tp'), may hold values from -0.09375 to 0.09375
- expert_down: bfloat16 [8, 1024, 4096], P('ep', 'tp'), may hold values from -0.1875 to 0.1875
Outputs:
- mixer_out: bfloat16 [4096, 4096], P(('ep', 'tp'))
- expert_out: bfloat16 [4096, 4096], P('ep', 'tp')
Inputs may be any that keep to these rules, and one draw needn't show every extreme that they name: `route_ids`: each row names two different experts of one group of 8 consecutive experts. On the rows of one device each group is named by exactly 512 rows, experts 2 i and 2 i + 1 together are named exactly 4 * 192 / 3 times, and no expert is named by more than 192 rows; one expert is named by exactly 192 rows of every device.
All inputs are finite; a program needn't handle non-finite values.
Results may differ from a plain program's by a relative error of at most 0.019.
Values may be sent and summed in bfloat16 or wider, within the bound.
A program may use at most 192 MiB of HBM per device.

v0:
```python
import functools

import jax
import jax.numpy as jnp
from jax import lax
from jax.experimental import pallas as pl
from jax.experimental.pallas import tpu as pltpu
from jax.sharding import PartitionSpec as P

BLOCK = 512
CHUNKS = 2


epsilon = 1e-06
theta_base = 10000.0
largest_entry = lax.Precision.HIGH


def prefix(state, decay, axis):
    length = lax.axis_size(axis)
    head_count, key_width, value_width = state.shape
    extra = 16

    def shifted(state, decay, distance):
        high = decay.astype(jnp.bfloat16)
        low = (decay - high.astype(jnp.float32)).astype(jnp.bfloat16)
        row = jnp.arange(extra)[None, :, None]
        tail = jnp.where(
            row == 0,
            high[:, None, None],
            jnp.where(row == 1, low[:, None, None], jnp.zeros((), jnp.bfloat16)),
        )
        packed = jnp.concatenate(
            [
                state.astype(jnp.bfloat16),
                jnp.broadcast_to(tail, (head_count, extra, value_width)),
            ],
            axis=1,
        )
        moved = lax.ppermute(
            packed, axis, [(i, i + distance) for i in range(length - distance)]
        ).astype(jnp.float32)
        return (moved[:, :key_width], moved[:, key_width, 0] + moved[:, key_width + 1, 0])

    if length == 1:
        return jnp.zeros_like(state)
    state, decay = shifted(state, decay, 1)
    distance = 1
    while distance < length - 1:
        earlier_state, earlier_decay = shifted(state, decay, distance)
        state = decay[:, None, None] * earlier_state + state
        decay = decay * earlier_decay
        distance *= 2
    return state


def rotate(values, positions):
    half_dim = values.shape[-1] // 2
    frequency = theta_base ** (-jnp.arange(half_dim, dtype=jnp.float32) / half_dim)
    angles = positions.astype(jnp.float32)[:, None, None] * frequency
    cosine = jnp.cos(angles)
    sine_wave = jnp.sin(angles)
    first_half = values[..., :half_dim]
    second = values[..., half_dim:]
    return jnp.concatenate(
        [first_half * cosine - second * sine_wave, second * cosine + first_half * sine_wave],
        axis=-1,
    )


def to_blocks(array, blocks):
    return array.reshape(blocks, array.shape[0] // blocks, array.shape[1], array.shape[2])


def retention_rows(queries, key_rows, value_rows, gate_rows, log_decay, head_gain, outgoing):
    length = queries.shape[0]
    head_count = log_decay.shape[0]
    key_width = queries.shape[1] // head_count
    value_width = value_rows.shape[1] // head_count
    blocks = length // BLOCK
    positions = lax.axis_index("ep") * length + jnp.arange(length, dtype=jnp.int32)
    query_rot = to_blocks(
        rotate(queries.astype(jnp.float32).reshape(length, head_count, key_width), positions),
        blocks,
    )
    key_rot = to_blocks(
        rotate(key_rows.astype(jnp.float32).reshape(length, head_count, key_width), positions)
        * key_width ** (-0.5),
        blocks,
    )
    value_all = to_blocks(
        value_rows.astype(jnp.float32).reshape(length, head_count, value_width), blocks
    )
    running = jnp.cumsum(log_decay.reshape(head_count, blocks, BLOCK), axis=2)
    ending = running[:, :, -1]
    kept = jnp.exp(ending[:, :, None] - running)
    block_states = jnp.einsum(
        "nlhd,hnl,nlhe->nhde", key_rot, kept, value_all, precision=lax.Precision.DEFAULT
    )
    block_decay = jnp.exp(ending).T

    def advance(carried, inputs):
        decay_now, state_now = inputs
        return (decay_now[:, None, None] * carried + state_now, carried)

    zeros_state = jnp.zeros((head_count, key_width, value_width), jnp.float32)
    device_state, local_starts = lax.scan(advance, zeros_state, (block_decay, block_states))
    device_decay = jnp.exp(jnp.sum(ending, axis=1))
    incoming = prefix(device_state, device_decay, "ep")
    incoming, outgoing = lax.optimization_barrier((incoming, outgoing))
    causal = jnp.arange(BLOCK)[:, None] >= jnp.arange(BLOCK)[None, :]
    spread = running[:, :, :, None] - running[:, :, None, :]
    weight_table = jnp.exp(jnp.where(causal, spread, -jnp.inf))
    score_matrix = (
        jnp.einsum("nlhd,nmhd->hnlm", query_rot, key_rot, precision=largest_entry) * weight_table
    )
    inside = jnp.einsum("hnlm,nmhe->nlhe", score_matrix, value_all, precision=lax.Precision.DEFAULT)
    before = jnp.exp(jnp.cumsum(ending, axis=1) - ending)
    starts = local_starts + before.T[:, :, None, None] * incoming[None]
    outside = jnp.einsum(
        "nlhd,hnl,nhde->nlhe", query_rot, jnp.exp(running), starts, precision=largest_entry
    )
    mixed = (inside + outside).reshape(length, head_count, value_width)
    centered = mixed - jnp.mean(mixed, axis=-1, keepdims=True)
    normed = (
        centered
        * lax.rsqrt(jnp.mean(centered * centered, axis=-1, keepdims=True) + epsilon)
        * head_gain.reshape(head_count, value_width)
    )
    hidden = (
        jax.nn.silu(gate_rows.astype(jnp.float32))
        * normed.reshape(length, head_count * value_width)
    ).astype(jnp.bfloat16)
    return (hidden, outgoing)


def return_kernel(n_ep, n_tp, width, src, dst, send_sem, recv_sem, local_sem):
    count = n_ep * n_tp
    me = lax.axis_index("ep") * n_tp + lax.axis_index("tp")

    def device(index):
        return (index // n_tp, lax.rem(index, n_tp))

    def block(index):
        owner, part = device(index)
        return src.at[owner, :, pl.ds(pl.multiple_of(part * width, width), width)]

    def copy(step):
        peer = lax.rem(me + step, count)
        return pltpu.make_async_remote_copy(
            src_ref=block(peer),
            dst_ref=dst.at[me],
            send_sem=send_sem.at[step],
            recv_sem=recv_sem.at[step],
            device_id=device(peer),
            device_id_type=pl.DeviceIdType.MESH,
        )

    def arrival(step):
        sender = lax.rem(me + count - step, count)
        return pltpu.make_async_remote_copy(
            src_ref=block(sender),
            dst_ref=dst.at[sender],
            send_sem=send_sem.at[step],
            recv_sem=recv_sem.at[step],
            device_id=device(sender),
            device_id_type=pl.DeviceIdType.MESH,
        )

    barrier = pltpu.get_barrier_semaphore()

    @pl.loop(1, count)
    def _(step):
        pl.semaphore_signal(
            barrier,
            inc=1,
            device_id=device(lax.rem(me + step, count)),
            device_id_type=pl.DeviceIdType.MESH,
        )

    own = pltpu.make_async_copy(block(me), dst.at[me], local_sem)
    own.start()
    pl.semaphore_wait(barrier, count - 1)

    @pl.loop(1, count)
    def _(step):
        copy(step).start()

    own.wait()

    @pl.loop(1, count)
    def _(step):
        copy(step).wait_send()
        arrival(step).wait_recv()


def send_back(finished, n_ep, n_tp, chunk):
    rows, width = finished.shape[1], finished.shape[2] // n_tp
    count = n_ep * n_tp
    return pl.pallas_call(
        functools.partial(return_kernel, n_ep, n_tp, width),
        out_shape=jax.ShapeDtypeStruct((count, rows, width), finished.dtype),
        in_specs=[pl.BlockSpec(memory_space=pl.ANY)],
        out_specs=pl.BlockSpec(memory_space=pl.ANY),
        scratch_shapes=[
            pltpu.SemaphoreType.DMA((count,)),
            pltpu.SemaphoreType.DMA((count,)),
            pltpu.SemaphoreType.DMA,
        ],
        compiler_params=pltpu.CompilerParams(collective_id=chunk, has_side_effects=True),
        cost_estimate=pl.CostEstimate(
            flops=40_000_000_000, bytes_accessed=2 * finished.size * 2, transcendentals=0
        ),
        name="send_back",
    )(finished)


def body(
    queries,
    key_rows,
    value_rows,
    gate_rows,
    log_decay,
    head_gain,
    out_weight,
    expert_input,
    input_gain,
    route_ids,
    route_weight,
    expert_gate,
    expert_up,
    expert_down,
):
    tp_count = lax.axis_size("tp")
    ep_count = lax.axis_size("ep")
    tp_index = lax.axis_index("tp")
    model_width = out_weight.shape[1]
    token_count = expert_input.shape[0]
    local_experts = expert_gate.shape[0]
    expert_count = ep_count * local_experts
    capacity = 3 * token_count // expert_count
    share = capacity // tp_count
    quarter = model_width // tp_count
    piece = quarter // CHUNKS
    unit_group = expert_down.shape[1]

    gate_whole = lax.all_gather(expert_gate, "tp", axis=2, tiled=True)
    up_whole = lax.all_gather(expert_up, "tp", axis=2, tiled=True)
    down_pieces = [
        jnp.concatenate(
            [
                lax.slice_in_dim(
                    expert_down, part * quarter + chunk * piece, part * quarter + (chunk + 1) * piece, axis=2
                )
                for part in range(tp_count)
            ],
            axis=2,
        )
        for chunk in range(CHUNKS)
    ]
    down_whole = [
        lax.all_gather(
            down_pieces[chunk],
            "tp",
            axis=1,
            tiled=True,
        )
        for chunk in range(CHUNKS)
    ]

    widened = expert_input.astype(jnp.float32)
    normed = (
        widened
        * lax.rsqrt(jnp.mean(widened * widened, axis=-1, keepdims=True) + epsilon)
        * input_gain
    ).astype(jnp.bfloat16)
    experts = jnp.arange(expert_count, dtype=jnp.int32)[None, :]
    named = [route_ids[:, k : k + 1] == experts for k in range(2)]
    both = (named[0] | named[1]).astype(jnp.bfloat16)
    order = jnp.arange(token_count, dtype=jnp.int32)
    earlier = (order[None, :] < order[:, None]).astype(jnp.bfloat16)
    ranks = jnp.dot(earlier, both, preferred_element_type=jnp.float32)
    code, place = [], []
    for k in range(2):
        ids = route_ids[:, k]
        rank = jnp.sum(jnp.where(named[k], ranks, 0.0), axis=1).astype(jnp.int32)
        code.append(ids * capacity + rank)
        place.append(
            (
                ((ids // local_experts) * tp_count + rank // share) * local_experts
                + ids % local_experts
            )
            * share
            + rank % share
        )
    slot = (
        experts[0][:, None] * capacity
        + tp_index * share
        + jnp.arange(share, dtype=jnp.int32)[None, :]
    ).reshape(-1, 1)
    chosen = ((slot == code[0][None, :]) | (slot == code[1][None, :])).astype(jnp.bfloat16)
    outgoing = jnp.dot(chosen, normed, preferred_element_type=jnp.float32).astype(jnp.bfloat16)
    hidden, outgoing = retention_rows(
        queries, key_rows, value_rows, gate_rows, log_decay, head_gain, outgoing
    )
    arrived = lax.all_to_all(
        outgoing.reshape(expert_count, share, model_width),
        "ep",
        split_axis=0,
        concat_axis=0,
        tiled=True,
    ).reshape(ep_count, local_experts, share, model_width)

    mixer_part = jnp.dot(hidden, out_weight, preferred_element_type=jnp.float32).astype(
        jnp.bfloat16
    )

    gate_val = jnp.einsum("sxcd,xdf->sxcf", arrived, gate_whole, preferred_element_type=jnp.float32)
    up_val = jnp.einsum("sxcd,xdf->sxcf", arrived, up_whole, preferred_element_type=jnp.float32)
    inner_rows = (jax.nn.silu(gate_val) * up_val).astype(jnp.bfloat16)

    slots = jnp.arange(expert_count * capacity, dtype=jnp.int32)[None, :]
    picks = (jnp.concatenate(place)[:, None] == slots).astype(jnp.bfloat16)
    returned = []
    for chunk in range(CHUNKS):
        if chunk > 0:
            inner_rows, returned[-1] = lax.optimization_barrier((inner_rows, returned[-1]))
        finished = (
            jnp.einsum(
                "sxcf,xfd->sxcd", inner_rows, down_whole[chunk], preferred_element_type=jnp.float32
            )
            .astype(jnp.bfloat16)
            .reshape(ep_count, local_experts * share, tp_count * piece)
        )
        if chunk == 0:
            finished, mixer_part = lax.optimization_barrier((finished, mixer_part))
        returned.append(send_back(finished, ep_count, tp_count, chunk))
    mixer_out = lax.psum_scatter(mixer_part, "tp", scatter_dimension=0, tiled=True)
    pieces = []
    for chunk in range(CHUNKS):
        rows = returned[chunk].reshape(expert_count * capacity, piece)
        picked = jnp.dot(picks, rows, preferred_element_type=jnp.float32)
        total = (
            picked[:token_count] * route_weight[:, :1] + picked[token_count:] * route_weight[:, 1:]
        )
        pieces.append(total.astype(jnp.bfloat16))
    expert_out = jnp.concatenate(pieces, axis=1)
    return (mixer_out, expert_out)


def solution(mesh):
    placed = (
        P("ep", "tp"),
        P("ep", "tp"),
        P("ep", "tp"),
        P("ep", "tp"),
        P("tp", "ep"),
        P("tp"),
        P("tp", None),
        P("ep", None),
        P(),
        P("ep", None),
        P("ep", None),
        P("ep", None, "tp"),
        P("ep", None, "tp"),
        P("ep", "tp", None),
    )
    return jax.shard_map(
        body,
        mesh=mesh,
        in_specs=placed,
        out_specs=(P(("ep", "tp"), None), P("ep", "tp")),
        check_vma=False,
    )
```

profile of v0, /device:TPU:0, one launch (start us, length us, event | category | flops | bytes accessed | tf_op | source)
XLA Modules:
  0.0 281.6 jit_solution(10795996751195244313)
XLA Ops:
  7.2 0.7 all-gather.7.cloned.1.call-update
  8.0 0.7 all-gather.9.cloned.1.call-update
  8.7 1.2 reduce-window.6
  10.9 1.3 copy.33
  12.4 0.5 multiply_cosine_fusion
  13.0 0.3 multiply_subtract_fusion
  13.3 0.9 copy-done.11
  14.2 0.6 fusion.58
  14.9 4.9 %collective-permute-start = (bf16[4,144,256]{2,1,0:T(8,128)(2,1)S(1)}, bf16[4,144,256]{2,1,0:T(8,128)(2,1)S(1)}, u32[]{:S(2)}, u32[]{:S(2)}) collective-permute-start(bf16[4,144,256]{2,1,0:T(8,128)(2,1)S(1)} %pad_maximum_fusion.6), channel_id=1, source_target_pairs={{0,4},{4,8},{8,12},{12,16},{16,20},{20,24},{24,28},{1,5},{5,9},{9,... | collective-permute-start | bytes 884744 | tf_op jit(solution)/shard_map/ppermute | solution.py:40
  20.0 1.1 pad_maximum_fusion
  21.1 3.9 %fusion = f32[512]{0:T(512)S(1)} fusion(bf16[512,4096]{1,0:T(8,128)(2,1)} %param.21), kind=kLoop, calls=%fused_computation.2 | loop fusion | flops 6290944 | bytes 4196352 | tf_op jit(solution)/shard_map/reduce_sum | solution.py:274
  25.1 0.9 collective-permute-done
  26.5 4.4 %collective-permute-start.1 = (bf16[4,144,256]{2,1,0:T(8,128)(2,1)S(1)}, bf16[4,144,256]{2,1,0:T(8,128)(2,1)S(1)}, u32[]{:S(2)}, u32[]{:S(2)}) collective-permute-start(bf16[4,144,256]{2,1,0:T(8,128)(2,1)S(1)} %pad_maximum_fusion.7), channel_id=1, source_target_pairs={{0,4},{4,8},{8,12},{12,16},{16,20},{20,24},{24,28},{1,5},{5,9},{9,... | collective-permute-start | bytes 884744 | tf_op jit(solution)/shard_map/ppermute | solution.py:40
  31.0 5.4 %collective-permute-done.1 = bf16[4,144,256]{2,1,0:T(8,128)(2,1)S(1)} collective-permute-done((bf16[4,144,256]{2,1,0:T(8,128)(2,1)S(1)}, bf16[4,144,256]{2,1,0:T(8,128)(2,1)S(1)}, u32[]{:S(2)}, u32[]{:S(2)}) %collective-permute-start.1) | collective-permute-done | bytes 294944 | tf_op jit(solution)/shard_map/ppermute | solution.py:40
  37.0 6.4 %collective-permute-start.2 = (bf16[4,144,256]{2,1,0:T(8,128)(2,1)S(1)}, bf16[4,144,256]{2,1,0:T(8,128)(2,1)S(1)}, u32[]{:S(2)}, u32[]{:S(2)}) collective-permute-start(bf16[4,144,256]{2,1,0:T(8,128)(2,1)S(1)} %pad_maximum_fusion.8), channel_id=1, source_target_pairs={{0,8},{4,12},{8,16},{12,20},{16,24},{20,28},{1,9},{5,13},{9,17},{1... | collective-permute-start | bytes 884744 | tf_op jit(solution)/shard_map/ppermute | solution.py:40
  43.5 0.3 select_reduce_fusion.1
  43.7 4.2 %collective-permute-done.2 = bf16[4,144,256]{2,1,0:T(8,128)(2,1)S(1)} collective-permute-done((bf16[4,144,256]{2,1,0:T(8,128)(2,1)S(1)}, bf16[4,144,256]{2,1,0:T(8,128)(2,1)S(1)}, u32[]{:S(2)}, u32[]{:S(2)}) %collective-permute-start.2) | collective-permute-done | bytes 294944 | tf_op jit(solution)/shard_map/ppermute | solution.py:40
  48.6 5.4 %collective-permute-start.3 = (bf16[4,144,256]{2,1,0:T(8,128)(2,1)S(1)}, bf16[4,144,256]{2,1,0:T(8,128)(2,1)S(1)}, u32[]{:S(2)}, u32[]{:S(2)}) collective-permute-start(bf16[4,144,256]{2,1,0:T(8,128)(2,1)S(1)} %pad_maximum_fusion.9), channel_id=1, source_target_pairs={{0,16},{4,20},{8,24},{12,28},{1,17},{5,21},{9,25},{13,29},{2,18},{... | collective-permute-start | bytes 884744 | tf_op jit(solution)/shard_map/ppermute | solution.py:40
  54.0 3.8 %convolution_convert_fusion.1 = bf16[384,4096]{1,0:T(8,128)(2,1)} fusion(bf16[512,4096]{1,0:T(8,128)(2,1)S(1)} %copy-done, f32[4096]{0:T(1024)S(1)} %copy-done.14, f32[512]{0:T(512)S(1)} %add_rsqrt_fusion.1, s32[512]{0:T(512)S(1)} %get-tuple-element.86, s32[512]{0:T(512)S(1)} %get-tuple-element.72, s32[384]{0:T(512)S(1)} %add.196), kind=kOutput, calls=%fused_computation.13 | convolution fusion | flops 1621164032 | bytes 7364096 | tf_op jit(solution)/shard_map/dot_general | solution.py:302
  57.8 0.4 collective-permute-done.3
  58.2 0.9 multiply_add_fusion.1
  59.1 11.4 %all-to-all-start = ((bf16[8,48,4096]{2,1,0:T(8,128)(2,1)}), bf16[8,48,4096]{2,1,0:T(8,128)(2,1)}, u32[]{:S(2)}, u32[]{:S(2)}) async-start(bf16[8,48,4096]{2,1,0:T(8,128)(2,1)} %bitcast.143), calls=%async_computation | async-start | bytes 6291456 | tf_op jit(solution)/shard_map/all_to_all | solution.py:306
  70.6 1.1 pad_maximum_fusion.2
  71.8 0.2 reduce-scatter.2.cloned.1.call-start
  72.1 1.9 fusion.74
  74.1 1.6 fusion.14
  75.8 1.3 fusion.127
  77.1 0.3 fusion.40
  77.5 0.6 mul.337
  78.1 1.8 copy.50
  80.0 1.6 sub.98
  81.6 3.3 %copy.41 = f32[512,1024]{1,0:T(8,128)} copy(f32[512,1024]{0,1:T(8,128)} %bitcast.140) | data formatting | bytes 4194304 | tf_op jit(solution)/shard_map/sub | solution.py:124
  84.9 1.8 copy.40
  86.7 12.3 %convolution_convert_fusion = bf16[512,4096]{1,0:T(8,128)(2,1)} fusion(bf16[1024,4096]{1,0:T(8,128)(2,1)} %param.20, f32[512,1024]{1,0:T(8,128)} %bitcast.144, f32[512,1024]{1,0:T(8,128)} %copy.40, f32[512,1024]{1,0:T(8,128)} %copy.41, bf16[512,1024]{1,0:T(8,128)(2,1)S(1)} %copy-done.13, f32[1024]{0:T(1024)S(1)} %copy-done.15), kind=kOutput, calls=%fused_computation.12 | convolution fusion | flops 4302307328 | bytes 19927040 | tf_op jit(solution)/shard_map/dot_general | solution.py:314
  99.0 42.3 %all-to-all-done = bf16[8,48,4096]{2,1,0:T(8,128)(2,1)} async-done(((bf16[8,48,4096]{2,1,0:T(8,128)(2,1)}), bf16[8,48,4096]{2,1,0:T(8,128)(2,1)}, u32[]{:S(2)}, u32[]{:S(2)}) %all-to-all-start) | async-done | bytes 3145760 | tf_op jit(solution)/shard_map/all_to_all | solution.py:306
  141.2 7.8 %fusion.5 = f32[8,48,1024]{2,1,0:T(8,128)S(1)} fusion(bf16[8,48,4096]{2,1,0:T(8,128)(2,1)} %all-to-all-done, bf16[1,4096,1024]{2,1,0:T(8,128)(2,1)} %all-gather.7.cloned.1.call-done), kind=kOutput, calls=%fused_computation.7 | convolution fusion | flops 3221225472 | bytes 13107200 | tf_op jit(solution)/shard_map/sxcd,xdf->sxcf/dot_general | solution.py:318
  149.0 7.9 %fusion.49 = bf16[8,1,48,1024]{3,2,0,1:T(8,128)(2,1)S(1)} fusion(f32[8,48,1024]{2,1,0:T(8,128)S(1)} %fusion.5, bf16[8,48,4096]{2,1,0:T(8,128)(2,1)} %all-to-all-done, bf16[1,4096,1024]{2,1,0:T(8,128)(2,1)} %all-gather.9.cloned.1.call-done), kind=kOutput, calls=%fused_computation.50 | convolution fusion | flops 3223584768 | bytes 13893632 | tf_op jit(solution)/shard_map/sxcd,xdf->sxcf/dot_general | solution.py:319
  157.0 12.3 %all-gather.5.cloned.1.call-done = bf16[1,1024,2048]{2,1,0:T(8,128)(2,1)} async-done(((bf16[1,256,2048]{2,1,0:T(8,128)(2,1)}), bf16[1,1024,2048]{2,1,0:T(8,128)(2,1)}) %all-gather.5.cloned.1.call-update) | async-done | bytes 4194320 | tf_op jit(solution)/shard_map/all_gather | solution.py:262
  169.3 5.1 %fusion.32.src = bf16[8,48,2048]{2,1,0:T(8,128)(2,1)} fusion(bf16[1,1024,2048]{2,1,0:T(8,128)(2,1)} %all-gather.5.cloned.1.call-done, bf16[8,1,48,1024]{3,2,0,1:T(8,128)(2,1)S(1)} %fusion.49), kind=kOutput, calls=%fused_computation.32 | convolution fusion | flops 1611399168 | bytes 6553600 | tf_op jit(solution)/shard_map/sxcf,xfd->sxcd/dot_general | solution.py:329
  174.5 31.3 %send_back.2 = bf16[32,48,512]{2,1,0:T(8,128)(2,1)} custom-call(bf16[8,48,2048]{2,1,0:T(8,128)(2,1)} %fusion.32.src), custom_call_target="tpu_custom_call" | custom-call | flops 40000000000 | bytes 3145728 | tf_op jit(solution)/shard_map/send_back/pallas_call | solution.py:200
  205.7 17.8 %all-gather.11.cloned.1.call-done = bf16[1,1024,2048]{2,1,0:T(8,128)(2,1)} async-done(((bf16[1,256,2048]{2,1,0:T(8,128)(2,1)}), bf16[1,1024,2048]{2,1,0:T(8,128)(2,1)}) %all-gather.11.cloned.1.call-update) | async-done | bytes 4194320 | tf_op jit(solution)/shard_map/all_gather | solution.py:262
  223.5 5.1 %fusion.29.src = bf16[8,48,2048]{2,1,0:T(8,128)(2,1)} fusion(bf16[1,1024,2048]{2,1,0:T(8,128)(2,1)} %all-gather.11.cloned.1.call-done, bf16[8,1,48,1024]{3,2,0,1:T(8,128)(2,1)S(1)} %fusion.49), kind=kOutput, calls=%fused_computation.31 | convolution fusion | flops 1611399168 | bytes 6553600 | tf_op jit(solution)/shard_map/sxcf,xfd->sxcd/dot_general | solution.py:329
  228.6 29.6 %send_back.3 = bf16[32,48,512]{2,1,0:T(8,128)(2,1)} custom-call(bf16[8,48,2048]{2,1,0:T(8,128)(2,1)} %fusion.29.src), custom_call_target="tpu_custom_call" | custom-call | flops 40000000000 | bytes 3145728 | tf_op jit(solution)/shard_map/send_back/pallas_call | solution.py:200
  258.2 3.5 %fusion.7 = f32[1024,512]{0,1:T(8,128)S(1)} fusion(bf16[1536,512]{1,0:T(8,128)(2,1)} %bitcast.161, s32[1024]{0:T(1024)S(1)} %pad_add_fusion), kind=kOutput, calls=%fused_computation.10 | convolution fusion | flops 1612185600 | bytes 3674112 | tf_op jit(solution)/shard_map/dot_general | solution.py:342
  261.8 2.1 fusion.8
  263.8 0.6 fusion.67
  264.5 1.3 copy.43
  265.8 9.3 %reduce-scatter.2.cloned.1.call-done = bf16[128,4096]{1,0:T(8,128)(2,1)} async-done(((bf16[512,4096]{1,0:T(8,128)(2,1)}), bf16[128,4096]{1,0:T(8,128)(2,1)}) %reduce-scatter.2.cloned.1.call-update) | async-done | bytes 1048592 | tf_op jit(solution)/shard_map/reduce_scatter | solution.py:338
  (96 shorter events, 3.9 us)
Async XLA Ops:
  7.2 1.6 copy-start.8
  7.2 3.5 %copy-start.7 = (bf16[512,512]{1,0:T(8,128)(2,1)S(1)}, bf16[512,512]{1,0:T(8,128)(2,1)}, u32[]{:S(2)}) copy-start(bf16[512,512]{1,0:T(8,128)(2,1)} %param.14) | copy-start | bytes 1572868
  7.2 134.1 %all-gather.7.cloned.1.call-start = ((), (), s32[]{:S(2)}) async-start(), calls=%async_computation.3 | async-start | bytes 10485760 | tf_op jit(solution)/shard_map/all_gather | solution.py:247
  7.9 141.1 %all-gather.9.cloned.1.call-start = ((), (), s32[]{:S(2)}) async-start(), calls=%async_computation.4 | async-start | bytes 10485760 | tf_op jit(solution)/shard_map/all_gather | solution.py:248
  8.7 160.6 %all-gather.5.cloned.1.call-start = ((), (), s32[]{:S(2)}) async-start(), calls=%async_computation.2 | async-start | bytes 5242880 | tf_op jit(solution)/shard_map/all_gather | solution.py:262
  13.0 1.2 copy-start.11
  13.3 6.7 %copy-start.1 = (f32[512,4,64]{0,2,1:T(8,128)}, f32[512,4,64]{0,2,1:T(8,128)S(1)}, u32[]{:S(2)}) copy-start(f32[512,4,64]{0,2,1:T(8,128)S(1)} %get-tuple-element.65) | copy-start | bytes 1572868
  13.3 6.7 %copy-start.3 = (f32[512,4,64]{0,2,1:T(8,128)}, f32[512,4,64]{0,2,1:T(8,128)S(1)}, u32[]{:S(2)}) copy-start(f32[512,4,64]{0,2,1:T(8,128)S(1)} %get-tuple-element.66) | copy-start | bytes 1572868
  13.3 6.5 %copy-start.6 = (bf16[1,256,4096]{2,1,0:T(8,128)(2,1)S(1)}, bf16[1,256,4096]{2,1,0:T(8,128)(2,1)}, u32[]{:S(2)}) copy-start(bf16[1,256,4096]{2,1,0:T(8,128)(2,1)} %param.27) | copy-start | bytes 6291460
  14.9 11.2 %collective-permute-start = (bf16[4,144,256]{2,1,0:T(8,128)(2,1)S(1)}, bf16[4,144,256]{2,1,0:T(8,128)(2,1)S(1)}, u32[]{:S(2)}, u32[]{:S(2)}) collective-permute-start(bf16[4,144,256]{2,1,0:T(8,128)(2,1)S(1)} %pad_maximum_fusion.6), channel_id=1, source_target_pairs={{0,4},{4,8},{8,12},{12,16},{16,20},{20,24},{24,28},{1,5},{5,9},{9,... | collective-permute-start | bytes 884744 | tf_op jit(solution)/shard_map/ppermute | solution.py:40
  21.1 9.9 %copy-start.9 = (s32[512,2]{0,1:T(2,128)S(1)}, s32[512,2]{0,1:T(2,128)}, u32[]{:S(2)}) copy-start(s32[512,2]{0,1:T(2,128)} %param.23) | copy-start | bytes 12292
  26.5 9.9 %collective-permute-start.1 = (bf16[4,144,256]{2,1,0:T(8,128)(2,1)S(1)}, bf16[4,144,256]{2,1,0:T(8,128)(2,1)S(1)}, u32[]{:S(2)}, u32[]{:S(2)}) collective-permute-start(bf16[4,144,256]{2,1,0:T(8,128)(2,1)S(1)} %pad_maximum_fusion.7), channel_id=1, source_target_pairs={{0,4},{4,8},{8,12},{12,16},{16,20},{20,24},{24,28},{1,5},{5,9},{9,... | collective-permute-start | bytes 884744 | tf_op jit(solution)/shard_map/ppermute | solution.py:40
  36.8 17.2 %copy-start = (bf16[512,4096]{1,0:T(8,128)(2,1)S(1)}, bf16[512,4096]{1,0:T(8,128)(2,1)}, u32[]{:S(2)}) copy-start(bf16[512,4096]{1,0:T(8,128)(2,1)} %param.21) | copy-start | bytes 12582916
  36.9 17.1 %copy-start.14 = (f32[4096]{0:T(1024)S(1)}, f32[4096]{0:T(1024)}, u32[]{:S(2)}) copy-start(f32[4096]{0:T(1024)} %param.22) | copy-start | bytes 49156
  37.0 10.9 %collective-permute-start.2 = (bf16[4,144,256]{2,1,0:T(8,128)(2,1)S(1)}, bf16[4,144,256]{2,1,0:T(8,128)(2,1)S(1)}, u32[]{:S(2)}, u32[]{:S(2)}) collective-permute-start(bf16[4,144,256]{2,1,0:T(8,128)(2,1)S(1)} %pad_maximum_fusion.8), channel_id=1, source_target_pairs={{0,8},{4,12},{8,16},{12,20},{16,24},{20,28},{1,9},{5,13},{9,17},{1... | collective-permute-start | bytes 884744 | tf_op jit(solution)/shard_map/ppermute | solution.py:40
  48.6 9.6 %collective-permute-start.3 = (bf16[4,144,256]{2,1,0:T(8,128)(2,1)S(1)}, bf16[4,144,256]{2,1,0:T(8,128)(2,1)S(1)}, u32[]{:S(2)}, u32[]{:S(2)}) collective-permute-start(bf16[4,144,256]{2,1,0:T(8,128)(2,1)S(1)} %pad_maximum_fusion.9), channel_id=1, source_target_pairs={{0,16},{4,20},{8,24},{12,28},{1,17},{5,21},{9,25},{13,29},{2,18},{... | collective-permute-start | bytes 884744 | tf_op jit(solution)/shard_map/ppermute | solution.py:40
  59.1 82.1 %all-to-all-start = ((bf16[8,48,4096]{2,1,0:T(8,128)(2,1)}), bf16[8,48,4096]{2,1,0:T(8,128)(2,1)}, u32[]{:S(2)}, u32[]{:S(2)}) async-start(bf16[8,48,4096]{2,1,0:T(8,128)(2,1)} %bitcast.143), calls=%async_computation | async-start | bytes 6291456 | tf_op jit(solution)/shard_map/all_to_all | solution.py:306
  70.6 1.4 copy-start.2
  70.6 1.5 copy-start.4
  70.6 152.9 %all-gather.11.cloned.1.call-start = ((), (), s32[]{:S(2)}) async-start(), calls=%async_computation.6 | async-start | bytes 5242880 | tf_op jit(solution)/shard_map/all_gather | solution.py:262
  71.8 203.3 %reduce-scatter.2.cloned.1.call-start = ((), (), s32[]{:S(2)}) async-start(), calls=%async_computation.5 | async-start | bytes 5242880 | tf_op jit(solution)/shard_map/reduce_scatter | solution.py:338
  72.1 2.0 copy-start.10
  72.1 2.0 copy-start.12
  74.1 1.6 copy-start.5
  84.9 1.8 copy-start.13
  84.9 1.8 copy-start.15
  258.2 3.6 %copy-start.16 = (bf16[32,48,512]{2,1,0:T(8,128)(2,1)S(1)}, bf16[32,48,512]{2,1,0:T(8,128)(2,1)}, u32[]{:S(2)}) copy-start(bf16[32,48,512]{2,1,0:T(8,128)(2,1)} %send_back.2) | copy-start | bytes 4718596
Sparse Core Ops, SparseCore 0:
  9.5 62.0 all-gather.6
  73.2 59.3 all-gather.8
  134.8 34.4 all-gather.4
  171.3 52.1 all-gather.10
  226.4 48.6 reduce-scatter.1
where the time goes:
time: 283 us; the launch traced here: 282 us
  waiting for transfers between devices  94 us (33%)
  Pallas kernels  60.8 us (21%)
  matrix products  53.3 us (19%)
  starting transfers between devices  33 us (12%)
  between operations  14.3 us (5%)
  local copies, waits for them, and re-layouts  14.2 us (5%)
  other arithmetic  12 us (4%)
    pallas_call x2, Pallas kernels, send_back(): pl.pallas_call(functools.partial(return_kernel, n_ep, n_tp, width), out_s...  60.8 us
    all_to_all x1, waiting for transfers between devices, body(): lax.all_to_all(outgoing.reshape(expert_count, share, model_width), 'ep',...  42.3 us
    all_gather x2, waiting for transfers between devices, body(): lax.all_gather(down_pieces[chunk], 'tp', axis=1, tiled=True)  30.1 us
    ppermute x4, starting transfers between devices, shifted(): lax.ppermute(packed, axis, [(i, i + distance) for i in range(length - dis...  21.2 us
    dot_general x1, matrix products, body(): jnp.dot(hidden, out_weight, preferred_element_type=jnp.float32)  12.3 us
    all_to_all x1, starting transfers between devices, body(): lax.all_to_all(outgoing.reshape(expert_count, share, model_width), 'ep',...  11.4 us
    ppermute x4, waiting for transfers between devices, shifted(): lax.ppermute(packed, axis, [(i, i + distance) for i in range(length - dis...  10.9 us
    dot_general x2, matrix products, body(): jnp.einsum('sxcf,xfd->sxcd', inner_rows, down_whole[chunk], preferred_ele...  10.3 us
  transfers between devices with their start and end apart: 10, of which 8 were waited for; matrix products, arithmetic and copies ran while one was open for 28% of the time, Pallas kernels for 22%

commit v1 on v0

v1 whole, which is shorter than its diff:
```python
import functools
import math

import jax
import jax.numpy as jnp
from jax import lax
from jax.experimental import pallas as pl
from jax.experimental.pallas import tpu as pltpu
from jax.sharding import PartitionSpec as P

MESH = pl.DeviceIdType.MESH
F32, BF16 = jnp.float32, jnp.bfloat16
epsilon = 1e-06
theta_base = 10000.0
TAIL = 16
LAG = 4


def xor(a, b, bits):
    total = 0
    for bit in range(bits):
        step = 1 << bit
        total = total + step * (((a // step) + (b // step)) % 2)
    return total


def dot(a, b, dims=((1,), (0,))):
    return lax.dot_general(a, b, (dims, ((), ())), preferred_element_type=F32)


def kernel(
    sizes,
    outgoing, gate, up, down, combine,
    queries, keys, values, gates, cosine, sine, run_col, run_row, gain, out_weight,
    mixer_out, expert_out,
    tok, gu, dn, wt, inn, res, ret,
    q_in, k_in, v_in, g_in, cos_s, sin_s, rc_s, rr_s, gain_s, ow,
    qhi, qlo, khi, klo, state, carry, packed, mixed, hidden, part, from_sib, from_far,
    acc,
    load_sem, ow_sem,
    disp_s, disp_r, tok_s, tok_r, inn_s, inn_r, ret_s, ret_r, dn_s, dn_r,
    chain_s, chain_r, mix_s, mix_r,
):
    n_ep, n_tp, heads, dk, dv = sizes
    bits = int(math.log2(n_ep))
    ep = lax.axis_index("ep")
    tp = lax.axis_index("tp")
    sib = xor(tp, 1, 2)
    far = xor(tp, 2, 2)
    diag = xor(tp, 3, 2)
    length = queries.shape[0]
    share, width = tok.shape[2], tok.shape[3]
    rows = n_tp * share
    units = gate.shape[2]
    cols = width // n_tp
    wide = ow.shape[2]
    n_wide = width // wide

    def local(k, src, dst):
        return pltpu.make_async_copy(src, dst, load_sem.at[k])

    def remote(src, dst, send, recv, device):
        return pltpu.make_async_remote_copy(
            src_ref=src, dst_ref=dst, send_sem=send, recv_sem=recv,
            device_id=device, device_id_type=MESH,
        )

    def dispatch(m):
        peer = xor(ep, m, bits)
        return remote(outgoing.at[peer], tok.at[ep, tp], disp_s.at[m], disp_r.at[m], (peer, tp))

    def dispatch_in(m):
        peer = xor(ep, m, bits)
        return remote(outgoing.at[peer], tok.at[peer, tp], disp_s.at[m], disp_r.at[m], (peer, tp))

    def own_rows():
        return pltpu.make_async_copy(outgoing.at[ep], tok.at[ep, tp], disp_r.at[0])

    def trade(ref, s, m, kind, send, recv, incoming=False):
        if incoming:
            piece = (far, sib, diag)[kind]
        else:
            piece = (tp, tp, far)[kind]
        device = (ep, (far, sib, sib)[kind])
        return remote(ref.at[s, piece], ref.at[s, piece], send.at[m, kind], recv.at[m, kind], device)

    def give_back(m):
        peer = xor(ep, m, bits)
        return remote(res.at[peer], ret.at[ep], ret_s.at[m], ret_r.at[m], (peer, tp))

    def give_back_in(m):
        peer = xor(ep, m, bits)
        return remote(res.at[peer], ret.at[peer], ret_s.at[m], ret_r.at[m], (peer, tp))

    def dn_out(j):
        peer = xor(tp, j, 2)
        start = pl.multiple_of(peer * cols, cols)
        return remote(down.at[0, :, pl.ds(start, cols)], dn.at[tp], dn_s.at[j], dn_r.at[j], (ep, peer))

    def dn_in(j):
        peer = xor(tp, j, 2)
        start = pl.multiple_of(peer * cols, cols)
        return remote(down.at[0, :, pl.ds(start, cols)], dn.at[peer], dn_s.at[j], dn_r.at[j], (ep, peer))

    def dn_own():
        start = pl.multiple_of(tp * cols, cols)
        return pltpu.make_async_copy(down.at[0, :, pl.ds(start, cols)], dn.at[tp], dn_r.at[0])

    def chain_out():
        return remote(packed, carry, chain_s, chain_r, (ep + 1, tp))

    def chain_in():
        return remote(packed, carry, chain_s, chain_r, (ep - 1, tp))

    def ow_copy(j, slot):
        start = pl.multiple_of(j * wide, wide)
        return pltpu.make_async_copy(out_weight.at[:, pl.ds(start, wide)], ow.at[slot], ow_sem.at[slot])

    def mix_copy(kind, incoming=False):
        if kind == 0:
            return remote(part.at[sib], from_sib.at[0], mix_s.at[0], mix_r.at[0], (ep, sib))
        if kind == 1:
            return remote(part.at[diag], from_sib.at[1], mix_s.at[1], mix_r.at[1], (ep, sib))
        return remote(part.at[far], from_far, mix_s.at[2], mix_r.at[2], (ep, far))

    loads = [
        local(0, queries, q_in), local(1, keys, k_in), local(2, values, v_in),
        local(3, gates, g_in), local(4, cosine, cos_s), local(5, sine, sin_s),
        local(6, run_col, rc_s), local(7, run_row, rr_s), local(8, gain, gain_s),
        local(9, gate.at[0], gu.at[:, pl.ds(0, units)]),
        local(10, up.at[0], gu.at[:, pl.ds(units, units)]),
        local(11, combine, wt),
    ]

    barrier = pltpu.get_barrier_semaphore()

    @pl.loop(1, n_ep)
    def _(m):
        pl.semaphore_signal(barrier, inc=1, device_id=(xor(ep, m, bits), tp), device_id_type=MESH)

    @pl.loop(1, n_tp)
    def _(j):
        pl.semaphore_signal(barrier, inc=1, device_id=(ep, xor(tp, j, 2)), device_id_type=MESH)

    for k in (0, 1, 2, 4, 5, 6, 7):
        loads[k].start()
    dn_own().start()
    own_rows().start()
    for k in (9, 10, 3, 8, 11):
        loads[k].start()
    for j in range(2):
        ow_copy(j, j).start()
    pl.semaphore_wait(barrier, n_ep - 1 + n_tp - 1)

    @pl.loop(0, n_ep - 1)
    def _(i):
        dispatch(n_ep - 1 - i).start()

    for j in range(1, n_tp):
        dn_out(j).start()

    def begin_retention():
        for k in (0, 1, 2, 4, 5, 6, 7):
            loads[k].wait()

        def turn(x):
            return x * cos_s[...] + pltpu.roll(x, dk // 2, 1) * sin_s[...]

        scale = dk ** -0.5
        for h in range(heads):
            lanes = slice(h * dk, (h + 1) * dk)
            q = turn(q_in[:, lanes].astype(F32))
            high = q.astype(BF16)
            qhi[h] = high
            qlo[h] = (q - high.astype(F32)).astype(BF16)
            k = turn(k_in[:, lanes].astype(F32)) * scale
            high = k.astype(BF16)
            khi[h] = high
            klo[h] = (k - high.astype(F32)).astype(BF16)
            col = rc_s[h]
            ending = col[length - 1 : length]
            kept = (k * jnp.exp(ending - col)).astype(BF16)
            state[h] = dot(kept, v_in[:, h * dv : (h + 1) * dv], ((0,), (0,)))

    def send_state():
        for h in range(heads):
            packed[h] = state[h].astype(BF16)
        chain_out().start()

    def pass_state():
        for h in range(heads):
            ending = rc_s[h][length - 1 : length]
            packed[h] = (jnp.exp(ending) * carry[h].astype(F32) + state[h]).astype(BF16)
        chain_out().start()

    def inside(h):
        vh = v_in[:, pl.ds(pl.multiple_of(h * dv, dv), dv)]
        col = rc_s[h]
        row = rr_s[h]
        step = min(length, 128)
        for r in range(length // step):
            lines = slice(r * step, (r + 1) * step)
            seen = (r + 1) * step
            nt = ((1,), (1,))
            score = (
                dot(qhi[h, lines], khi[h, :seen], nt)
                + dot(qhi[h, lines], klo[h, :seen], nt)
                + dot(qlo[h, lines], khi[h, :seen], nt)
            )
            later = lax.broadcasted_iota(jnp.int32, (step, seen), 0) + r * step
            earlier = lax.broadcasted_iota(jnp.int32, (step, seen), 1)
            spread = col[lines] - row[:, :seen]
            weight = jnp.exp(jnp.where(later >= earlier, spread, -jnp.inf))
            mixed[h, lines] = dot((score * weight).astype(BF16), vh[:seen])

    def finish_retention():
        loads[3].wait()
        loads[8].wait()
        step = min(length, 128)
        chunks = length // step

        @pl.loop(0, heads * chunks)
        def _(c):
            h = c // chunks
            lines = pl.ds(pl.multiple_of((c % chunks) * step, step), step)
            lanes = pl.ds(pl.multiple_of(h * dv, dv), dv)
            begun = carry[h]
            outside = dot(qhi[h, lines], begun) + dot(qlo[h, lines], begun)
            o = mixed[h, lines] + outside * jnp.exp(rc_s[h, lines])
            centered = o - jnp.mean(o, axis=1, keepdims=True)
            normed = (
                centered
                * lax.rsqrt(jnp.mean(centered * centered, axis=1, keepdims=True) + epsilon)
                * gain_s[:, lanes]
            )
            g = g_in[lines, lanes].astype(F32)
            hidden[lines, lanes] = (g / (1.0 + jnp.exp(-g)) * normed).astype(BF16)

        @pl.loop(0, n_wide)
        def _(j):
            slot = j % 2
            ow_copy(j, slot).wait()
            total = dot(hidden[...], ow[slot]).astype(BF16)
            here = pl.ds(pl.multiple_of(j * wide, wide), wide)
            part[:, :, here] = total.reshape(n_tp, length // n_tp, wide)

            @pl.when(j + 2 < n_wide)
            def _():
                ow_copy(j + 2, slot).start()

        mix_copy(1).start()
        mix_copy(0).start()

    def forward_mix():
        mix_copy(1).wait_send()
        mix_copy(1).wait_recv()
        part[far] = (part[far].astype(F32) + from_sib[1].astype(F32)).astype(BF16)
        mix_copy(2).start()

    @pl.loop(0, n_ep + LAG)
    def _(i):
        @pl.when(i < n_ep)
        def _():
            m = n_ep - 1 - i
            s = xor(ep, m, bits)

            @pl.when(m > 0)
            def _():
                dispatch_in(m).wait_recv()

            @pl.when(m == 0)
            def _():
                own_rows().wait()

            trade(tok, s, m, 0, tok_s, tok_r).start()
            trade(tok, s, m, 1, tok_s, tok_r).start()

        @pl.when((i >= 1) & (i < n_ep + 1))
        def _():
            m = n_ep - i
            s = xor(ep, m, bits)
            trade(tok, s, m, 0, tok_s, tok_r, True).wait_recv()
            trade(tok, s, m, 2, tok_s, tok_r).start()

        @pl.when(i == 0)
        def _():
            begin_retention()

            @pl.when(ep == 0)
            def _():
                carry[...] = jnp.zeros_like(carry)
                send_state()

        @pl.when((i == ep) & (ep > 0))
        def _():
            chain_in().wait_recv()

            @pl.when(ep < n_ep - 1)
            def _():
                pass_state()

        @pl.when((i >= 1) & (i < 1 + heads))
        def _():
            inside(i - 1)

        @pl.when(i == 1)
        def _():
            loads[9].wait()
            loads[10].wait()

        @pl.when((i >= 2) & (i < n_ep + 2))
        def _():
            m = n_ep + 1 - i
            s = xor(ep, m, bits)
            trade(tok, s, m, 1, tok_s, tok_r, True).wait_recv()
            trade(tok, s, m, 2, tok_s, tok_r, True).wait_recv()
            both = dot(tok[s].reshape(rows, width), gu[...])
            g = both[:, :units]
            inn[s, tp] = (g / (1.0 + jnp.exp(-g)) * both[:, units:]).astype(BF16)
            trade(inn, s, m, 0, inn_s, inn_r).start()
            trade(inn, s, m, 1, inn_s, inn_r).start()

        @pl.when((i >= 3) & (i < n_ep + 3))
        def _():
            m = n_ep + 2 - i
            s = xor(ep, m, bits)
            trade(inn, s, m, 0, inn_s, inn_r, True).wait_recv()
            trade(inn, s, m, 2, inn_s, inn_r).start()

        @pl.when(i == 3)
        def _():
            dn_own().wait()
            for j in range(1, n_tp):
                dn_in(j).wait_recv()

        @pl.when(i >= 4)
        def _():
            m = n_ep + 3 - i
            s = xor(ep, m, bits)
            trade(inn, s, m, 1, inn_s, inn_r, True).wait_recv()
            trade(inn, s, m, 2, inn_s, inn_r, True).wait_recv()
            total = dot(inn[s, 0], dn[0])
            for t in range(1, n_tp):
                total = total + dot(inn[s, t], dn[t])
            res[s] = total.astype(BF16)

            @pl.when(m > 0)
            def _():
                give_back(m).start()

        @pl.when(i == n_ep)
        def _():
            finish_retention()

        @pl.when(i == n_ep + 2)
        def _():
            forward_mix()

    loads[11].wait()
    acc[...] = dot(wt[ep], res[ep], ((0,), (0,)))

    @pl.loop(0, n_ep - 1)
    def _(i):
        m = n_ep - 1 - i
        s = xor(ep, m, bits)
        give_back_in(m).wait_recv()
        acc[...] += dot(wt[s], ret[s], ((0,), (0,)))

    expert_out[...] = acc[...].astype(BF16)

    mix_copy(0).wait_recv()
    mix_copy(2).wait_recv()
    mixer_out[...] = (
        part[tp].astype(F32) + from_sib[0].astype(F32) + from_far[...].astype(F32)
    ).astype(BF16)

    mix_copy(0).wait_send()
    mix_copy(2).wait_send()

    @pl.when(ep < n_ep - 1)
    def _():
        chain_out().wait_send()

    for j in range(1, n_tp):
        dn_out(j).wait_send()

    @pl.loop(0, n_ep)
    def _(m):
        s = xor(ep, m, bits)
        for kind in range(3):
            trade(tok, s, m, kind, tok_s, tok_r).wait_send()
            trade(inn, s, m, kind, inn_s, inn_r).wait_send()

    @pl.loop(1, n_ep)
    def _(m):
        dispatch(m).wait_send()
        give_back(m).wait_send()


def body(
    queries, key_rows, value_rows, gate_rows, log_decay, head_gain, out_weight,
    expert_input, input_gain, route_ids, route_weight, expert_gate, expert_up, expert_down,
):
    n_tp = lax.axis_size("tp")
    n_ep = lax.axis_size("ep")
    tp_index = lax.axis_index("tp")
    width = out_weight.shape[1]
    tokens = expert_input.shape[0]
    n_experts = n_ep * expert_gate.shape[0]
    units = expert_gate.shape[2]
    capacity = 3 * tokens // n_experts
    share = -(-capacity // (n_tp * 16)) * 16
    rows = share * n_tp
    cols = width // n_tp
    length = queries.shape[0]
    heads = log_decay.shape[0]
    dk = queries.shape[1] // heads
    dv = value_rows.shape[1] // heads

    widened = expert_input.astype(F32)
    normed = (
        widened
        * lax.rsqrt(jnp.mean(widened * widened, axis=-1, keepdims=True) + epsilon)
        * input_gain
    ).astype(BF16)
    experts = jnp.arange(n_experts, dtype=jnp.int32)[None, :]
    named = [route_ids[:, k : k + 1] == experts for k in range(2)]
    both = (named[0] | named[1]).astype(BF16)
    order = jnp.arange(tokens, dtype=jnp.int32)
    earlier = (order[None, :] < order[:, None]).astype(BF16)
    ranks = jnp.dot(earlier, both, preferred_element_type=F32)
    code = [
        route_ids[:, k] * rows
        + jnp.sum(jnp.where(named[k], ranks, 0.0), axis=1).astype(jnp.int32)
        for k in range(2)
    ]
    slot = (
        experts[0][:, None] * rows
        + tp_index * share
        + jnp.arange(share, dtype=jnp.int32)[None, :]
    ).reshape(-1, 1)
    chosen = ((slot == code[0][None, :]) | (slot == code[1][None, :])).astype(BF16)
    outgoing = (
        jnp.dot(chosen, normed, preferred_element_type=F32)
        .astype(BF16)
        .reshape(n_experts, share, width)
    )
    slots = jnp.arange(n_experts * rows, dtype=jnp.int32)[:, None]
    combine = (
        jnp.where(slots == code[0][None, :], route_weight[None, :, 0], 0.0)
        + jnp.where(slots == code[1][None, :], route_weight[None, :, 1], 0.0)
    ).astype(BF16).reshape(n_experts, rows, tokens)

    positions = lax.axis_index("ep") * length + jnp.arange(length, dtype=jnp.int32)
    half = dk // 2
    frequency = theta_base ** (-jnp.arange(half, dtype=F32) / half)
    angles = positions.astype(F32)[:, None] * frequency
    cosine, sine = jnp.cos(angles), jnp.sin(angles)
    cosine = jnp.concatenate([cosine, cosine], axis=1)
    sine = jnp.concatenate([-sine, sine], axis=1)
    running = jnp.cumsum(log_decay, axis=1)

    wide = 512
    sizes = (n_ep, n_tp, heads, dk, dv)
    any_spec = pl.BlockSpec(memory_space=pl.ANY)
    vmem = pl.BlockSpec(memory_space=pltpu.VMEM)
    dma = pltpu.SemaphoreType.DMA
    mixer_out, expert_out = pl.pallas_call(
        functools.partial(kernel, sizes),
        out_shape=(
            jax.ShapeDtypeStruct((length // n_tp, width), BF16),
            jax.ShapeDtypeStruct((tokens, cols), BF16),
        ),
        in_specs=[any_spec] * 15,
        out_specs=(vmem, vmem),
        scratch_shapes=[
            pltpu.VMEM((n_ep, n_tp, share, width), BF16),
            pltpu.VMEM((width, 2 * units), BF16),
            pltpu.VMEM((n_tp, units, cols), BF16),
            pltpu.VMEM((n_experts, rows, tokens), BF16),
            pltpu.VMEM((n_ep, n_tp, rows, units), BF16),
            pltpu.VMEM((n_ep, rows, cols), BF16),
            pltpu.VMEM((n_ep, rows, cols), BF16),
            pltpu.VMEM((length, heads * dk), BF16),
            pltpu.VMEM((length, heads * dk), BF16),
            pltpu.VMEM((length, heads * dv), BF16),
            pltpu.VMEM((length, heads * dv), BF16),
            pltpu.VMEM((length, dk), F32),
            pltpu.VMEM((length, dk), F32),
            pltpu.VMEM((heads, length, 1), F32),
            pltpu.VMEM((heads, 1, length), F32),
            pltpu.VMEM((1, heads * dv), F32),
            pltpu.VMEM((2, heads * dv, wide), BF16),
            pltpu.VMEM((heads, length, dk), BF16),
            pltpu.VMEM((heads, length, dk), BF16),
            pltpu.VMEM((heads, length, dk), BF16),
            pltpu.VMEM((heads, length, dk), BF16),
            pltpu.VMEM((heads, dk, dv), F32),
            pltpu.VMEM((heads, dk, dv), BF16),
            pltpu.VMEM((heads, dk, dv), BF16),
            pltpu.VMEM((heads, length, dv), F32),
            pltpu.VMEM((length, heads * dv), BF16),
            pltpu.VMEM((n_tp, length // n_tp, width), BF16),
            pltpu.VMEM((2, length // n_tp, width), BF16),
            pltpu.VMEM((length // n_tp, width), BF16),
            pltpu.VMEM((tokens, cols), F32),
            dma((12,)),
            dma((2,)),
            dma((n_ep,)), dma((n_ep,)),
            dma((n_ep, 3)), dma((n_ep, 3)),
            dma((n_ep, 3)), dma((n_ep, 3)),
            dma((n_ep,)), dma((n_ep,)),
            dma((n_tp,)), dma((n_tp,)),
            dma, dma,
            dma((3,)), dma((3,)),
        ],
        compiler_params=pltpu.CompilerParams(
            collective_id=0, has_side_effects=True, vmem_limit_bytes=67_043_328
        ),
        name="fused",
    )(
        outgoing, expert_gate, expert_up, expert_down, combine,
        queries, key_rows, value_rows, gate_rows, cosine, sine,
        running[:, :, None], running[:, None, :], head_gain[None, :], out_weight,
    )
    return (mixer_out, expert_out)


def solution(mesh):
    placed = (
        P("ep", "tp"),
        P("ep", "tp"),
        P("ep", "tp"),
        P("ep", "tp"),
        P("tp", "ep"),
        P("tp"),
        P("tp", None),
        P("ep", None),
        P(),
        P("ep", None),
        P("ep", None),
        P("ep", None, "tp"),
        P("ep", None, "tp"),
        P("ep", "tp", None),
    )
    return jax.shard_map(
        body,
        mesh=mesh,
        in_specs=placed,
        out_specs=(P(("ep", "tp"), None), P("ep", "tp")),
        check_vma=False,
    )
```

time: 283 us -> 205 us (0.72)
  Pallas kernels: 60.8 us -> 182 us
  waiting for transfers between devices: 94 us -> 0 us
  matrix products: 53.3 us -> 6.15 us
  starting transfers between devices: 33 us -> 0 us
  between operations: 14.3 us -> 0.76 us
  local copies, waits for them, and re-layouts: 14.2 us -> 6.69 us
  other arithmetic: 12 us -> 8.44 us
    pallas_call x2 -> x1, Pallas kernels: 60.8 us -> 182 us  [body(): pl.pallas_call(functools.partial(kernel, sizes), out_shape=(jax.ShapeDtyp...]
    dot_general x13 -> x2, matrix products: 53.3 us -> 6.15 us  [the longest x1 5.9 us: body(): jnp.dot(chosen, normed, preferred_element_type=F32).astype(BF16)]
    all_to_all x1 -> x0, waiting for transfers between devices: 42.3 us -> none  [body(): lax.all_to_all(outgoing.reshape(expert_count, share, model_width), 'ep',...]
    all_gather x4 -> x0, waiting for transfers between devices: 30.1 us -> none  [the longest x2 30.1 us: body(): lax.all_gather(down_pieces[chunk], 'tp', axis=1, tiled=True)]
    ppermute x4 -> x0, starting transfers between devices: 21.2 us -> none  [shifted(): lax.ppermute(packed, axis, [(i, i + distance) for i in range(length - dis...]
    all_to_all x1 -> x0, starting transfers between devices: 11.4 us -> none  [body(): lax.all_to_all(outgoing.reshape(expert_count, share, model_width), 'ep',...]
    ppermute x4 -> x0, waiting for transfers between devices: 10.9 us -> none  [shifted(): lax.ppermute(packed, axis, [(i, i + distance) for i in range(length - dis...]
    reduce_scatter x1 -> x0, waiting for transfers between devices: 9.3 us -> none  [body(): lax.psum_scatter(mixer_part, 'tp', scatter_dimension=0, tiled=True)]
  transfers between devices with their start and end apart: 10 -> 0, of which waited for: 8 -> 0; matrix products, arithmetic and copies ran while one was open for 28% -> 0% of each run, Pallas kernels for 22% -> 0%
where the time goes in v1:
time: 205 us
  Pallas kernels  182 us (89%)
  other arithmetic  8.44 us (4%)
  local copies, waits for them, and re-layouts  6.69 us (3%)
  matrix products  6.15 us (3%)
    pallas_call x1, Pallas kernels, body(): pl.pallas_call(functools.partial(kernel, sizes), out_shape=(jax.ShapeDtyp...  182 us
    dot_general x1, matrix products, body(): jnp.dot(chosen, normed, preferred_element_type=F32).astype(BF16)  5.9 us
    unnamed x12, local copies, waits for them, and re-layouts  4.57 us

profile of v1, /device:TPU:0, one launch (start us, length us, event | category | flops | bytes accessed | tf_op | source)
XLA Modules:
  0.0 204.5 jit_solution(13697498068404421871)
XLA Ops:
  0.6 0.0 copy-start.3
  0.6 0.0 copy-start.2
  0.7 0.0 copy-start.1
  0.7 3.1 %fusion = f32[512]{0:T(512)S(1)} fusion(bf16[512,4096]{1,0:T(8,128)(2,1)} %param.21), kind=kLoop, calls=%fused_computation.2 | loop fusion | flops 6290944 | bytes 4196352 | tf_op jit(solution)/shard_map/reduce_sum | solution.py:423
  3.8 0.0 copy-start.4
  3.8 0.1 iota_add_fusion
  3.9 0.1 add.80
  4.0 0.0 copy-done.2
  4.0 0.3 select_reduce_fusion.1
  4.3 0.0 copy-done.3
  4.3 0.0 copy-done.1
  4.3 1.2 reduce-window.6
  5.5 0.2 slice_reduce_fusion
  5.7 0.2 reduce-window.9
  5.9 0.1 broadcast_add_fusion
  5.9 0.0 copy-start
  6.0 1.0 fusion.13
  7.0 1.0 pad_maximum_fusion
  8.0 1.9 reduce_window_sum.34.run_col
  9.8 1.8 add_convert_fusion.combine
  11.6 0.0 copy-done.4
  11.6 5.9 %convolution_convert_fusion = bf16[384,4096]{1,0:T(8,128)(2,1)} fusion(bf16[512,4096]{1,0:T(8,128)(2,1)} %param.21, f32[4096]{0:T(1024)S(1)} %copy-done.4, f32[512]{0:T(512)S(1)} %add_rsqrt_fusion, s32[512]{0:T(512)S(1)} %get-tuple-element.11, s32[512]{0:T(512)S(1)} %get-tuple-element.12, s32[384]{0:T(512)S(1)} %add.80), kind=kOutput, calls=%fused_computation.5 | convolution fusion | flops 1621164032 | bytes 7364096 | tf_op jit(solution)/shard_map/dot_general | solution.py:444
  17.5 0.0 copy-done
  17.5 182.5 %fused.1 = (bf16[128,4096]{1,0:T(8,128)(2,1)}, bf16[512,1024]{1,0:T(8,128)(2,1)}) custom-call(bf16[8,48,4096]{2,1,0:T(8,128)(2,1)} %bitcast.8, bf16[1,4096,256]{2,1,0:T(8,128)(2,1)} %gate.1, bf16[1,4096,256]{2,1,0:T(8,128)(2,1)} %up.1, bf16[1,256,4096]{2,1,0:T(8,128)(2,1)} %down.1, bf16[8,192,512]{2,1,0:T(8,128)(2,1)} %add_convert_fusion.combine, ...), custom_call_target="tpu_custom_call" | custom-call | tf_op jit(solution)/shard_map/fused/pallas_call | solution.py:468
  200.0 2.3 %copy.19 = bf16[128,4096]{1,0:T(8,128)(2,1)} copy(bf16[128,4096]{1,0:T(8,128)(2,1)} %get-tuple-element.17) | data formatting | bytes 2097152
  202.2 2.3 %copy.20 = bf16[512,1024]{1,0:T(8,128)(2,1)} copy(bf16[512,1024]{1,0:T(8,128)(2,1)} %get-tuple-element.18) | data formatting | bytes 2097152
  (9 shorter events, 0.1 us)
Async XLA Ops:
  0.6 3.6 %copy-start.3 = (f32[512,2]{0,1:T(2,128)S(1)}, f32[512,2]{0,1:T(2,128)}, u32[]{:S(2)}) copy-start(f32[512,2]{0,1:T(2,128)} %param.24) | copy-start | bytes 12292
  0.6 3.3 %copy-start.2 = (s32[512,2]{0,1:T(2,128)S(1)}, s32[512,2]{0,1:T(2,128)}, u32[]{:S(2)}) copy-start(s32[512,2]{0,1:T(2,128)} %param.23) | copy-start | bytes 12292
  0.7 3.6 %copy-start.1 = (f32[4,512]{1,0:T(4,128)S(1)}, f32[4,512]{1,0:T(4,128)}, u32[]{:S(2)}) copy-start(f32[4,512]{1,0:T(4,128)} %param.18) | copy-start | bytes 24580
  3.8 7.8 %copy-start.4 = (f32[4096]{0:T(1024)S(1)}, f32[4096]{0:T(1024)}, u32[]{:S(2)}) copy-start(f32[4096]{0:T(1024)} %param.22) | copy-start | bytes 49156
  5.9 11.5 %copy-start = (f32[4,4,128]{2,1,0:T(4,128)}, f32[4,4,128]{2,1,0:T(4,128)S(1)}, u32[]{:S(2)}) copy-start(f32[4,4,128]{2,1,0:T(4,128)S(1)} %broadcast_add_fusion) | copy-start | bytes 24580

commit v2 on v1

v2 whole, which is shorter than its diff:
```python
import functools
import math

import jax
import jax.numpy as jnp
import numpy as np
from jax import lax
from jax.experimental import pallas as pl
from jax.experimental.pallas import tpu as pltpu
from jax.sharding import PartitionSpec as P

MESH = pl.DeviceIdType.MESH
F32, BF16 = jnp.float32, jnp.bfloat16
epsilon = 1e-06
theta_base = 10000.0
LAG = 2
NEAR = 2
WHOLE = 2


def xor(a, b, bits):
    total = 0
    for bit in range(bits):
        step = 1 << bit
        total = total + step * (((a // step) + (b // step)) % 2)
    return total


def dot(a, b, dims=((1,), (0,))):
    return lax.dot_general(a, b, (dims, ((), ())), preferred_element_type=F32)


NT = ((1,), (1,))
TN = ((0,), (0,))


def silu(g):
    return g / (1.0 + jnp.exp(-g))


def kernel(
    sizes,
    expert_in, in_gain, ids, weights, gate, up, down,
    queries, keys, values, gates, cos_near, sin_near, cos_base, sin_base, decay, gain, out_weight,
    mixer_out, expert_out,
    xp, ig_s, ids_s, w_s, code_s, sel, outg, tok, oth, gu, dn, inn_a, inn_b, res_a, res_b, theirs, merged, ret,
    counts, count_out,
    q_in, k_in, v_in, g_in, cos_s, sin_s, cb_s, sb_s, ld_s, rc_s, rr_s, gain_s, ow,
    qhi, qlo, khi, klo, state, carry, packed, even_out, even_in, end_out, end_in, mixed, hidden, from_sib, from_far,
    load_sem, ow_sem,
    disp_s, disp_r, cnt_s, cnt_r, tok_s, tok_r, y_s, y_r, yf_s, yf_r,
    ia_s, ia_r, ib_s, ib_r, mg_s, mg_r, ret_s, ret_r, dn_s, dn_r,
    chain_s, chain_r, even_s, even_r, mix_s, mix_r,
):
    n_ep, n_tp, heads, dk, dv = sizes
    pairs = n_ep // 2
    ep_bits, pair_bits = int(math.log2(n_ep)), int(math.log2(pairs))
    ep = lax.axis_index("ep")
    tp = lax.axis_index("tp")
    pair, par = ep // 2, ep % 2
    mate = xor(ep, 1, 1) + pair * 2
    sib = xor(tp, 1, 2)
    far = xor(tp, 2, 2)
    diag = xor(tp, 3, 2)
    length = queries.shape[0]
    tokens, width = expert_in.shape[0] * expert_in.shape[1], expert_in.shape[2]
    block = tok.shape[1]
    chunk = block // n_tp
    cap = oth.shape[1]
    units = gate.shape[2]
    cols = width // n_tp
    wide = ow.shape[2]
    n_wide = width // wide
    half = width // 2
    side = pl.ds(pl.multiple_of((tp % 2) * half, half), half)
    mine = pl.ds(pl.multiple_of(par * chunk, chunk), cap)
    needed = pl.ds(pl.multiple_of((1 - par) * chunk, chunk), cap)

    def local(k, src, dst):
        return pltpu.make_async_copy(src, dst, load_sem.at[k])

    def remote(src, dst, send, recv, device):
        return pltpu.make_async_remote_copy(
            src_ref=src, dst_ref=dst, send_sem=send, recv_sem=recv,
            device_id=device, device_id_type=MESH,
        )

    def peer_of(m):
        return xor(pair, m, pair_bits)

    outer = (pair == 0) | (pair == pairs - 1)

    def block_at(i):
        late = jnp.where(i == pairs - 1, 1, i + 1)
        return jnp.where(i == 0, 0, jnp.where(outer, late, jnp.where(i == 1, 1, pairs + 1 - i)))

    def send_order(i):
        return jnp.where((i < 2) | ~outer, i, pairs + 1 - i)

    def rows_of(piece):
        return pl.ds(pl.multiple_of(piece * chunk, chunk), chunk)

    def lanes_of(hv):
        return slice(hv * half, (hv + 1) * half)

    def dispatch(m, which, hv):
        return remote(
            outg.at[m + which * pairs, :, lanes_of(hv)],
            tok.at[m, rows_of((tp, far)[which]), lanes_of(hv)],
            disp_s.at[m, which, hv], disp_r.at[m, which, hv], (peer_of(m) * 2 + par, tp),
        )

    def own_rows(which, hv):
        return pltpu.make_async_copy(
            outg.at[which * pairs, :, lanes_of(hv)],
            tok.at[0, rows_of((tp, far)[which]), lanes_of(hv)], disp_r.at[0, which, hv],
        )

    def count_copy(m):
        return remote(count_out, counts.at[m], cnt_s.at[m], cnt_r.at[m], (xor(ep, m, ep_bits), tp))

    def trade_tok(m, kind, hv, incoming=False):
        piece = rows_of(((far, sib, diag) if incoming else (tp, tp, far))[kind])
        device = (ep, (far, sib, sib)[kind])
        there = tok.at[m, piece, lanes_of(hv)]
        return remote(there, there, tok_s.at[m, kind, hv], tok_r.at[m, kind, hv], device)

    def trade(ref, send, recv, m, kind, incoming=False):
        piece = ((far, sib, diag) if incoming else (tp, tp, far))[kind]
        device = (ep, (far, sib, sib)[kind])
        return remote(ref.at[m, piece], ref.at[m, piece], send.at[m, kind], recv.at[m, kind], device)

    def cross(m):
        return remote(tok.at[m, needed, side], oth.at[m, :, side], y_s.at[m], y_r.at[m], (mate, tp))

    def cross_on(m, incoming=False):
        if incoming:
            there = pl.ds(pl.multiple_of((1 - tp % 2) * half, half), half)
        else:
            there = side
        return remote(oth.at[m, :, there], oth.at[m, :, there], yf_s.at[m, 0], yf_r.at[m, 0], (ep, sib))

    def quarter(piece):
        return pl.ds(pl.multiple_of(piece * cols, cols), cols)

    def cross_part(m):
        there = quarter(tp)
        return remote(
            tok.at[m, needed, there], oth.at[m, :, there], y_s.at[m], y_r.at[m], (mate, tp)
        )

    def share(m, kind, incoming=False):
        there = oth.at[m, :, quarter(((far, sib, diag) if incoming else (tp, tp, far))[kind])]
        device = (ep, (far, sib, sib)[kind])
        return remote(there, there, yf_s.at[m, kind], yf_r.at[m, kind], device)

    def to_mate(m):
        return remote(res_b.at[m], theirs.at[m], mg_s.at[m], mg_r.at[m], (mate, tp))

    def give_back(m):
        return remote(merged.at[m], ret.at[m], ret_s.at[m], ret_r.at[m], (peer_of(m) * 2 + par, tp))

    def dn_copy(j, incoming=False):
        peer = xor(tp, j, 2)
        start = pl.multiple_of(peer * cols, cols)
        return remote(
            down.at[0, :, pl.ds(start, cols)], dn.at[peer if incoming else tp],
            dn_s.at[j], dn_r.at[j], (ep, peer),
        )

    def dn_own():
        start = pl.multiple_of(tp * cols, cols)
        return pltpu.make_async_copy(down.at[0, :, pl.ds(start, cols)], dn.at[tp], dn_r.at[0])

    def chain(k):
        return remote(packed, carry, chain_s.at[k], chain_r, ((pair + 1) * 2 + k, tp))

    def even_copies():
        return (
            remote(even_out, even_in, even_s.at[0], even_r.at[0], (mate, tp)),
            remote(end_out, end_in, even_s.at[1], even_r.at[1], (mate, tp)),
        )

    def ow_copy(j, slot):
        start = pl.multiple_of(j * wide, wide)
        return pltpu.make_async_copy(out_weight.at[:, pl.ds(start, wide)], ow.at[slot], ow_sem.at[slot])

    def mix_copy(kind):
        if kind == 0:
            return remote(xp.at[sib], from_sib.at[0], mix_s.at[0], mix_r.at[0], (ep, sib))
        if kind == 1:
            return remote(xp.at[diag], from_sib.at[1], mix_s.at[1], mix_r.at[1], (ep, sib))
        return remote(xp.at[far], from_far, mix_s.at[2], mix_r.at[2], (ep, far))

    loads = [
        local(0, queries, q_in), local(1, keys, k_in), local(2, values, v_in),
        local(3, gates, g_in), local(4, cos_near, cos_s), local(5, sin_near, sin_s),
        local(6, cos_base, cb_s), local(7, sin_base, sb_s), local(8, decay, ld_s),
        local(9, gain, gain_s),
        local(10, gate.at[0], gu.at[:, pl.ds(0, units)]),
        local(11, up.at[0], gu.at[:, pl.ds(units, units)]),
        local(12, expert_in, xp), local(13, in_gain, ig_s), local(14, ids, ids_s),
        local(15, weights, w_s),
    ]

    def begin_retention():
        for k in (0, 1, 2, 4, 5, 6, 7, 8):
            loads[k].wait()
        older = lax.broadcasted_iota(jnp.int32, (length, length), 0)
        newer = lax.broadcasted_iota(jnp.int32, (length, length), 1)
        upper = (older <= newer).astype(BF16)
        lower = (newer <= older).astype(BF16)
        left = ld_s[...]
        run_row = jnp.zeros((heads, length), F32)
        run_col = jnp.zeros((length, heads), F32)
        for _ in range(3):
            piece = left.astype(BF16)
            run_row = run_row + dot(piece, upper)
            run_col = run_col + dot(lower, piece, NT)
            left = left - piece.astype(F32)
        lane = lax.broadcasted_iota(jnp.int32, (1, dk), 1)
        sign = jnp.where(lane < dk // 2, -1.0, 1.0)
        near_cos, near_sin = cos_s[...], sin_s[...]
        base_cos, base_sin = cb_s[ep], sb_s[ep]
        cosine = near_cos * base_cos - near_sin * base_sin
        sine = (near_sin * base_cos + near_cos * base_sin) * sign

        def turn(x):
            return x * cosine + pltpu.roll(x, dk // 2, 1) * sine

        scale = dk ** -0.5
        for h in range(heads):
            lanes = slice(h * dk, (h + 1) * dk)
            q = turn(q_in[:, lanes].astype(F32))
            high = q.astype(BF16)
            qhi[h] = high
            qlo[h] = (q - high.astype(F32)).astype(BF16)
            k = turn(k_in[:, lanes].astype(F32)) * scale
            high = k.astype(BF16)
            khi[h] = high
            klo[h] = (k - high.astype(F32)).astype(BF16)
            col = run_col[:, h : h + 1]
            rc_s[h] = col
            rr_s[h] = run_row[h : h + 1]
            ending = col[length - 1 : length]
            kept = (k * jnp.exp(ending - col)).astype(BF16)
            local_state = dot(kept, v_in[:, h * dv : (h + 1) * dv], TN)
            state[h] = local_state
            even_out[h] = local_state.astype(BF16)
            end_out[h : h + 1] = jnp.broadcast_to(ending, (1, 128))

    barrier = pltpu.get_barrier_semaphore()

    @pl.loop(1, n_ep)
    def _(m):
        pl.semaphore_signal(
            barrier, inc=1, device_id=(xor(ep, m, ep_bits), tp), device_id_type=MESH
        )

    @pl.loop(1, n_tp)
    def _(j):
        pl.semaphore_signal(barrier, inc=1, device_id=(ep, xor(tp, j, 2)), device_id_type=MESH)

    for k in (14, 13, 12, 15, 8, 0, 1, 2, 4, 5, 6, 7):
        loads[k].start()
    dn_own().start()
    for k in (10, 11, 3, 9):
        loads[k].start()
    for j in range(2):
        ow_copy(j, j).start()

    loads[14].wait()
    lanes = lax.broadcasted_iota(jnp.int32, (tokens, 128), 1)
    named = [(ids_s[:, k : k + 1] == lanes).astype(F32) for k in range(2)]
    both = named[0] + named[1]
    order = lax.broadcasted_iota(jnp.int32, (tokens, tokens), 0)
    before = lax.broadcasted_iota(jnp.int32, (tokens, tokens), 1)
    ranks = dot((before < order).astype(BF16), both.astype(BF16))
    total = jnp.sum(both, axis=0, keepdims=True)
    count_out[...] = jnp.broadcast_to(total, count_out.shape)
    code = []
    for k in range(2):
        rank = jnp.sum(named[k] * ranks, axis=1, keepdims=True)
        e = ids_s[:, k : k + 1]
        lower = jnp.where((lanes + 1 == e) & (e % 2 == 1), 1.0, 0.0)
        ahead = jnp.sum(lower * total, axis=1, keepdims=True)
        code.append((e // 2).astype(F32) * block + rank + ahead)
    code_s[...] = jnp.where(lanes == 0, code[0], jnp.where(lanes == 1, code[1], 0.0))
    flipped = code_s[...].T
    slot = lax.broadcasted_iota(jnp.int32, (chunk, 1), 0)
    for n in range(pairs + NEAR):
        first = peer_of(n % pairs) * block + (tp, far)[n // pairs] * chunk
        at = (slot + first).astype(F32)
        sel[n] = ((at == flipped[0:1]) | (at == flipped[1:2])).astype(BF16)

    begin_retention()
    pl.semaphore_wait(barrier, n_ep - 1 + n_tp - 1)

    @pl.when(par == 0)
    def _():
        for copy in even_copies():
            copy.start()

    for j in range(1, n_tp):
        dn_copy(j).start()

    @pl.loop(1, n_ep)
    def _(m):
        count_copy(m).start()

    counts[0] = count_out[...]
    loads[13].wait()
    loads[12].wait()
    part_rows = xp.shape[1]
    step = min(part_rows, 32)

    for part in range(n_tp):

        @pl.loop(0, part_rows // step)
        def _(c):
            at = pl.ds(pl.multiple_of(c * step, step), step)
            x = xp[part, at].astype(F32)
            scale = lax.rsqrt(jnp.mean(x * x, axis=1, keepdims=True) + epsilon)
            xp[part, at] = (x * scale * ig_s[...]).astype(BF16)

    @pl.loop(0, n_wide)
    def _(j):
        here = pl.ds(pl.multiple_of(j * wide, wide), wide)
        rows = xp[:, :, here].reshape(tokens, wide)
        chosen = sel[...].reshape((pairs + NEAR) * chunk, tokens)
        outg[:, :, here] = dot(chosen, rows).astype(BF16).reshape(pairs + NEAR, chunk, wide)

    for hv in range(2):
        for which in range(2):
            own_rows(which, hv).start()

    @pl.loop(1, pairs)
    def _(i):
        m = send_order(i)
        for hv in range(2):
            dispatch(m, 0, hv).start()

            @pl.when(m < NEAR)
            def _():
                dispatch(m, 1, hv).start()

    def pass_state():
        for copy in even_copies():
            copy.wait_recv()
        for h in range(heads):
            last = rc_s[h][length - 1 : length]
            first = end_in[h : h + 1, 0:1]
            earlier = carry[h].astype(F32)
            before = even_in[h].astype(F32)
            packed[h] = (
                jnp.exp(first + last) * earlier + jnp.exp(last) * before + state[h]
            ).astype(BF16)
            carry[h] = (jnp.exp(first) * earlier + before).astype(BF16)

        @pl.when(pair < pairs - 1)
        def _():
            chain(0).start()
            chain(1).start()

    def take_state():
        @pl.when(pair > 0)
        def _():
            chain(0).wait_recv()

        @pl.when(par == 1)
        def _():
            pass_state()

    def inside(h):
        lanes = pl.ds(pl.multiple_of(h * dv, dv), dv)
        vh = v_in[:, lanes]
        col = rc_s[h]
        row = rr_s[h]
        step = min(length, 128)
        for r in range(length // step):
            lines = slice(r * step, (r + 1) * step)
            seen = (r + 1) * step
            score = (
                dot(qhi[h, lines], khi[h, :seen], NT)
                + dot(qhi[h, lines], klo[h, :seen], NT)
                + dot(qlo[h, lines], khi[h, :seen], NT)
            )
            later = lax.broadcasted_iota(jnp.int32, (step, seen), 0) + r * step
            earlier = lax.broadcasted_iota(jnp.int32, (step, seen), 1)
            spread = col[lines] - row[:, :seen]
            weight = jnp.exp(jnp.where(later >= earlier, spread, -jnp.inf))
            mixed[lines, lanes] = dot((score * weight).astype(BF16), vh[:seen])

    def finish_retention():
        loads[3].wait()
        loads[9].wait()
        step = min(length, 128)
        parts = length // step

        @pl.loop(0, heads * parts)
        def _(c):
            h = c // parts
            lines = pl.ds(pl.multiple_of((c % parts) * step, step), step)
            lanes = pl.ds(pl.multiple_of(h * dv, dv), dv)
            begun = carry[h]
            outside = dot(qhi[h, lines], begun) + dot(qlo[h, lines], begun)
            o = mixed[lines, lanes] + outside * jnp.exp(rc_s[h, lines])
            centered = o - jnp.mean(o, axis=1, keepdims=True)
            normed = (
                centered
                * lax.rsqrt(jnp.mean(centered * centered, axis=1, keepdims=True) + epsilon)
                * gain_s[:, lanes]
            )
            hidden[lines, lanes] = (silu(g_in[lines, lanes].astype(F32)) * normed).astype(BF16)

        @pl.loop(0, n_wide)
        def _(j):
            slot = j % 2
            ow_copy(j, slot).wait()
            total = dot(hidden[...], ow[slot]).astype(BF16)
            here = pl.ds(pl.multiple_of(j * wide, wide), wide)
            xp[:, :, here] = total.reshape(n_tp, length // n_tp, wide)

            @pl.when(j + 2 < n_wide)
            def _():
                ow_copy(j + 2, slot).start()

        mix_copy(1).start()
        mix_copy(0).start()

    def forward_mix():
        mix_copy(1).wait_send()
        mix_copy(1).wait_recv()
        xp[far] = (xp[far].astype(F32) + from_sib[1].astype(F32)).astype(BF16)
        mix_copy(2).start()

    line = lax.broadcasted_iota(jnp.int32, (cap, 1), 0).astype(F32) + (par * chunk).astype(F32)
    odd = par.astype(F32)

    def hide(rows, m, other):
        both = dot(rows, gu[...])
        inner = silu(both[:, :units]) * both[:, units:]
        source = 2 * m + other
        tile = counts[source][0:1]
        lane = lax.broadcasted_iota(jnp.int32, tile.shape, 1)
        even = jnp.sum(jnp.where(lane == 2 * pair, tile, 0.0), axis=1, keepdims=True)
        keep = (line < even).astype(F32)
        keep = keep * (1.0 - 2.0 * odd) + odd
        return jnp.where(keep > 0.5, inner, 0.0).astype(BF16)

    def finish(inn, m):
        total = dot(inn[m, 0], dn[0])
        for t in range(1, n_tp):
            total = total + dot(inn[m, t], dn[t])
        return total.astype(BF16)

    def arrive(m):
        for hv in range(2):
            @pl.when(m > 0)
            def _():
                dispatch(m, 0, hv).wait_recv()

            @pl.when(m == 0)
            def _():
                own_rows(0, hv).wait()
                own_rows(1, hv).wait()

            @pl.when(m >= NEAR)
            def _():
                trade_tok(m, 0, hv).start()

            trade_tok(m, 1, hv).start()

            @pl.when((m > 0) & (m < NEAR))
            def _():
                dispatch(m, 1, hv).wait_recv()

            @pl.when(m < NEAR)
            def _():
                trade_tok(m, 2, hv).start()

    def merge(m):
        to_mate(m).wait_recv()

        @pl.when(par == 0)
        def _():
            merged[m, :chunk] = res_a[m, :chunk]
            merged[m, chunk:cap] = res_a[m, chunk:] + theirs[m, : cap - chunk]
            merged[m, cap:] = theirs[m, cap - chunk :]

        @pl.when(par == 1)
        def _():
            merged[m, :chunk] = theirs[m, :chunk]
            merged[m, chunk:cap] = theirs[m, chunk:] + res_a[m, : cap - chunk]
            merged[m, cap:] = res_a[m, cap - chunk :]

        @pl.when(m > 0)
        def _():
            give_back(m).start()

    def spread(m, hv, late):
        @pl.when(m >= NEAR)
        def _():
            trade_tok(m, 0, hv, True).wait_recv()
            trade_tok(m, 2, hv).start()

        trade_tok(m, 1, hv, True).wait_recv()
        trade_tok(m, 2, hv, True).wait_recv()

        @pl.when(jnp.logical_not(late) & (tp % 2 == hv))
        def _():
            cross(m).start()

        @pl.when(late & (tp // 2 == hv))
        def _():
            cross_part(m).start()

    arrive(jnp.int32(0))

    @pl.loop(0, pairs + LAG)
    def _(i):
        @pl.when(i < pairs)
        def _():
            m = block_at(i)
            spread(m, 0, i >= WHOLE)
            spread(m, 1, i >= WHOLE)

            @pl.when(i == 0)
            def _():
                loads[10].wait()
                loads[11].wait()

            @pl.when(m > 0)
            def _():
                count_copy(2 * m).wait_recv()

            inn_a[m, tp] = hide(tok[m, mine], m, 0)
            trade(inn_a, ia_s, ia_r, m, 0).start()
            trade(inn_a, ia_s, ia_r, m, 1).start()

        @pl.when(i == 0)
        def _():
            @pl.when(pair == 0)
            def _():
                carry[...] = jnp.zeros_like(carry)

            @pl.loop(0, heads)
            def _(h):
                inside(h)

        @pl.when(((i == 0) & (pair == 0)) | ((i == pair + 1) & (pair > 0) & (pair < pairs - 1)))
        def _():
            take_state()

        @pl.when((i - 1 >= WHOLE) & (i < pairs + 1))
        def _():
            m = block_at(i - 1)
            cross_part(m).wait_recv()
            share(m, 0).start()
            share(m, 1).start()

        @pl.when(i < pairs - 1)
        def _():
            arrive(block_at(i + 1))

        @pl.when(i == pairs - 1)
        def _():
            @pl.when(pair == pairs - 1)
            def _():
                take_state()

            finish_retention()

        @pl.when(i == pairs)
        def _():
            merge(block_at(i - 2))

        @pl.when(i == 1)
        def _():
            dn_own().wait()
            for j in range(1, n_tp):
                dn_copy(j, True).wait_recv()

        @pl.when((i >= 1) & (i < pairs + 1))
        def _():
            m = block_at(i - 1)
            trade(inn_a, ia_s, ia_r, m, 0, True).wait_recv()
            trade(inn_a, ia_s, ia_r, m, 2).start()

            @pl.when(i - 1 < WHOLE)
            def _():
                cross(m).wait_recv()
                cross_on(m).start()
                cross_on(m, True).wait_recv()

            @pl.when(i - 1 >= WHOLE)
            def _():
                share(m, 0, True).wait_recv()
                share(m, 2).start()
                share(m, 1, True).wait_recv()
                share(m, 2, True).wait_recv()

            count_copy(2 * m + 1).wait_recv()
            inn_b[m, tp] = hide(oth[m], m, 1)
            trade(inn_b, ib_s, ib_r, m, 0).start()
            trade(inn_b, ib_s, ib_r, m, 1).start()

            @pl.when(i == pairs)
            def _():
                forward_mix()

            trade(inn_a, ia_s, ia_r, m, 1, True).wait_recv()
            trade(inn_a, ia_s, ia_r, m, 2, True).wait_recv()
            res_a[m] = finish(inn_a, m)
            trade(inn_b, ib_s, ib_r, m, 0, True).wait_recv()
            trade(inn_b, ib_s, ib_r, m, 2).start()
            trade(inn_b, ib_s, ib_r, m, 1, True).wait_recv()
            trade(inn_b, ib_s, ib_r, m, 2, True).wait_recv()
            res_b[m] = finish(inn_b, m)
            to_mate(m).start()

        @pl.when((i >= 2) & (i != pairs))
        def _():
            merge(block_at(i - 2))

    loads[15].wait()
    place = lax.broadcasted_iota(jnp.int32, (tokens, block), 1).astype(F32)

    def combine(m, rows):
        at = code_s[...] - (peer_of(m) * block).astype(F32)
        pick = jnp.where(place == at[:, 0:1], w_s[:, 0:1], 0.0) + jnp.where(
            place == at[:, 1:2], w_s[:, 1:2], 0.0
        )
        return dot(pick.astype(BF16), rows)

    mixed[...] = combine(0, merged[0])

    mix_copy(0).wait_recv()
    mix_copy(2).wait_recv()
    mixer_out[...] = (
        xp[tp].astype(F32) + from_sib[0].astype(F32) + from_far[...].astype(F32)
    ).astype(BF16)

    @pl.loop(0, pairs - 1)
    def _(i):
        m = block_at(i + 1)
        give_back(m).wait_recv()
        mixed[...] += combine(m, ret[m])

    expert_out[...] = mixed[...].astype(BF16)

    mix_copy(0).wait_send()
    mix_copy(2).wait_send()

    @pl.when((par == 1) & (pair < pairs - 1))
    def _():
        chain(0).wait_send()
        chain(1).wait_send()

    @pl.when(par == 0)
    def _():
        for copy in even_copies():
            copy.wait_send()

    for j in range(1, n_tp):
        dn_copy(j).wait_send()

    @pl.loop(0, pairs)
    def _(i):
        m = block_at(i)
        for hv in range(2):
            @pl.when(m >= NEAR)
            def _():
                trade_tok(m, 0, hv).wait_send()

            trade_tok(m, 1, hv).wait_send()
            trade_tok(m, 2, hv).wait_send()

        for kind in range(3):
            trade(inn_a, ia_s, ia_r, m, kind).wait_send()
            trade(inn_b, ib_s, ib_r, m, kind).wait_send()

        @pl.when(i < WHOLE)
        def _():
            cross(m).wait_send()
            cross_on(m).wait_send()

        @pl.when(i >= WHOLE)
        def _():
            cross_part(m).wait_send()
            for kind in range(3):
                share(m, kind).wait_send()

        to_mate(m).wait_send()

    @pl.loop(1, pairs)
    def _(m):
        for hv in range(2):
            dispatch(m, 0, hv).wait_send()

            @pl.when(m < NEAR)
            def _():
                dispatch(m, 1, hv).wait_send()

        give_back(m).wait_send()

    @pl.loop(1, n_ep)
    def _(m):
        count_copy(m).wait_send()


def body(
    queries, key_rows, value_rows, gate_rows, log_decay, head_gain, out_weight,
    expert_input, input_gain, route_ids, route_weight, expert_gate, expert_up, expert_down,
):
    n_tp = lax.axis_size("tp")
    n_ep = lax.axis_size("ep")
    width = out_weight.shape[1]
    tokens = expert_input.shape[0]
    n_experts = n_ep * expert_gate.shape[0]
    units = expert_gate.shape[2]
    capacity = 3 * tokens // n_experts
    block = 4 * capacity // 3
    chunk = block // n_tp
    pairs = n_ep // 2
    cols = width // n_tp
    length = queries.shape[0]
    heads = log_decay.shape[0]
    dk = queries.shape[1] // heads
    dv = value_rows.shape[1] // heads
    assert tokens == length and cols == heads * dv

    half = dk // 2
    frequency = theta_base ** (-np.arange(half) / half)
    frequency = np.concatenate([frequency, frequency])
    near = np.arange(length)[:, None] * frequency
    base = (np.arange(n_ep) * length)[:, None, None] * frequency
    tables = [jnp.asarray(f(a), F32) for a in (near, base) for f in (np.cos, np.sin)]

    wide = 512
    sizes = (n_ep, n_tp, heads, dk, dv)
    any_spec = pl.BlockSpec(memory_space=pl.ANY)
    vmem = pl.BlockSpec(memory_space=pltpu.VMEM)
    dma = pltpu.SemaphoreType.DMA
    V = pltpu.VMEM
    mixer_out, expert_out = pl.pallas_call(
        functools.partial(kernel, sizes),
        out_shape=(
            jax.ShapeDtypeStruct((length // n_tp, width), BF16),
            jax.ShapeDtypeStruct((tokens, cols), BF16),
        ),
        in_specs=[any_spec] * 18,
        out_specs=(vmem, vmem),
        scratch_shapes=[
            V((n_tp, tokens // n_tp, width), BF16),
            V((1, width), F32),
            V((tokens, 2), jnp.int32),
            V((tokens, 2), F32),
            V((tokens, 128), F32),
            V((pairs + NEAR, chunk, tokens), BF16),
            V((pairs + NEAR, chunk, width), BF16),
            V((pairs, block, width), BF16),
            V((pairs, capacity, width), BF16),
            V((width, 2 * units), BF16),
            V((n_tp, units, cols), BF16),
            V((pairs, n_tp, capacity, units), BF16),
            V((pairs, n_tp, capacity, units), BF16),
            V((pairs, capacity, cols), BF16),
            V((pairs, capacity, cols), BF16),
            V((pairs, capacity, cols), BF16),
            V((pairs, block, cols), BF16),
            V((pairs, block, cols), BF16),
            V((n_ep, 8, 128), F32),
            V((8, 128), F32),
            V((length, heads * dk), BF16),
            V((length, heads * dk), BF16),
            V((length, heads * dv), BF16),
            V((length, heads * dv), BF16),
            V((length, dk), F32),
            V((length, dk), F32),
            V((n_ep, 1, dk), F32),
            V((n_ep, 1, dk), F32),
            V((heads, length), F32),
            V((heads, length, 1), F32),
            V((heads, 1, length), F32),
            V((1, heads * dv), F32),
            V((2, heads * dv, wide), BF16),
            V((heads, length, dk), BF16),
            V((heads, length, dk), BF16),
            V((heads, length, dk), BF16),
            V((heads, length, dk), BF16),
            V((heads, dk, dv), F32),
            V((heads, dk, dv), BF16),
            V((heads, dk, dv), BF16),
            V((heads, dk, dv), BF16),
            V((heads, dk, dv), BF16),
            V((8, 128), F32),
            V((8, 128), F32),
            V((length, heads * dv), F32),
            V((length, heads * dv), BF16),
            V((2, length // n_tp, width), BF16),
            V((length // n_tp, width), BF16),
            dma((16,)),
            dma((2,)),
            dma((pairs, 2, 2)), dma((pairs, 2, 2)),
            dma((n_ep,)), dma((n_ep,)),
            dma((pairs, 3, 2)), dma((pairs, 3, 2)),
            dma((pairs,)), dma((pairs,)),
            dma((pairs, 3)), dma((pairs, 3)),
            dma((pairs, 3)), dma((pairs, 3)),
            dma((pairs, 3)), dma((pairs, 3)),
            dma((pairs,)), dma((pairs,)),
            dma((pairs,)), dma((pairs,)),
            dma((n_tp,)), dma((n_tp,)),
            dma((2,)), dma,
            dma((2,)), dma((2,)),
            dma((3,)), dma((3,)),
        ],
        compiler_params=pltpu.CompilerParams(
            collective_id=0, has_side_effects=True, vmem_limit_bytes=67_043_328
        ),
        name="fused",
    )(
        expert_input.reshape(n_tp, tokens // n_tp, width), input_gain[None, :],
        route_ids, route_weight, expert_gate, expert_up, expert_down,
        queries, key_rows, value_rows, gate_rows, tables[0], tables[1], tables[2], tables[3],
        log_decay, head_gain[None, :], out_weight,
    )
    return (mixer_out, expert_out)


def solution(mesh):
    placed = (
        P("ep", "tp"),
        P("ep", "tp"),
        P("ep", "tp"),
        P("ep", "tp"),
        P("tp", "ep"),
        P("tp"),
        P("tp", None),
        P("ep", None),
        P(),
        P("ep", None),
        P("ep", None),
        P("ep", None, "tp"),
        P("ep", None, "tp"),
        P("ep", "tp", None),
    )
    return jax.shard_map(
        body,
        mesh=mesh,
        in_specs=placed,
        out_specs=(P(("ep", "tp"), None), P("ep", "tp")),
        check_vma=False,
    )
```

time: 205 us -> 188 us (0.917)
  other arithmetic: 8.44 us -> 0 us
  matrix products: 6.15 us -> 0 us
    dot_general x2 -> x0, matrix products: 6.15 us -> none  [the longest x1 5.9 us: body(): jnp.dot(chosen, normed, preferred_element_type=F32).astype(BF16)]
    reduce_sum x1 -> x0, other arithmetic: 3.08 us -> none  [body(): jnp.mean(widened * widened, axis=-1, keepdims=True) + epsilon]
    unnamed x12 -> x6, local copies, waits for them, and re-layouts: 4.57 us -> 6.43 us
where the time goes in v2:
time: 188 us
  Pallas kernels  181 us (96%)
  local copies, waits for them, and re-layouts  6.43 us (3%)
    pallas_call x1, Pallas kernels, body(): pl.pallas_call(functools.partial(kernel, sizes), out_shape=(jax.ShapeDtyp...  181 us
    unnamed x6, local copies, waits for them, and re-layouts  6.43 us

profile of v2, /device:TPU:0, one launch (start us, length us, event | category | flops | bytes accessed | tf_op | source)
XLA Modules:
  0.0 188.1 jit_solution(4595968208731327609)
XLA Ops:
  0.6 1.5 copy.20.ids
  2.2 1.5 copy.21.weights
  3.7 181.1 %fused.1 = (bf16[128,4096]{1,0:T(8,128)(2,1)}, bf16[512,1024]{1,0:T(8,128)(2,1)}) custom-call(bf16[4,128,4096]{2,1,0:T(8,128)(2,1)} %bitcast.3, f32[1,4096]{1,0:T(1,128)} %bitcast.4, s32[512,2]{1,0:T(8,128)} %copy.20.ids, f32[512,2]{1,0:T(8,128)} %copy.21.weights, bf16[1,4096,256]{2,1,0:T(8,128)(2,1)} %gate.1, bf16[1,4096,256]{2,1,0:T(8,128)(2,1)} %up.1, ...), custom_call_target="tpu_custom_call" | custom-call | tf_op jit(solution)/shard_map/fused/pallas_call | solution.py:746
  184.8 0.0 copy-start
  184.8 2.4 %copy.24 = bf16[128,4096]{1,0:T(8,128)(2,1)} copy(bf16[128,4096]{1,0:T(8,128)(2,1)} %get-tuple-element.4) | data formatting | bytes 2097152
  187.2 0.0 copy-done
  187.2 1.0 copy.25
Async XLA Ops:
  184.8 2.4 %copy-start = (bf16[512,1024]{1,0:T(8,128)(2,1)S(1)}, bf16[512,1024]{1,0:T(8,128)(2,1)}, u32[]{:S(2)}) copy-start(bf16[512,1024]{1,0:T(8,128)(2,1)} %get-tuple-element.5) | copy-start | bytes 3145732

commit v3 on v2

--- a/solution.py
+++ b/solution.py
@@ -362,15 +362,6 @@
             chain(0).start()
             chain(1).start()
 
-    def take_state():
-        @pl.when(pair > 0)
-        def _():
-            chain(0).wait_recv()
-
-        @pl.when(par == 1)
-        def _():
-            pass_state()
-
     def inside(h):
         lanes = pl.ds(pl.multiple_of(h * dv, dv), dv)
         vh = v_in[:, lanes]
@@ -548,9 +539,15 @@
             def _(h):
                 inside(h)
 
-        @pl.when(((i == 0) & (pair == 0)) | ((i == pair + 1) & (pair > 0) & (pair < pairs - 1)))
-        def _():
-            take_state()
+        @pl.when(((i == 0) & (pair == 0)) | ((i == pair + 1) & (pair > 0)))
+        def _():
+            @pl.when(pair > 0)
+            def _():
+                chain(0).wait_recv()
+
+            @pl.when(par == 1)
+            def _():
+                pass_state()
 
         @pl.when((i - 1 >= WHOLE) & (i < pairs + 1))
         def _():
@@ -563,16 +560,9 @@
         def _():
             arrive(block_at(i + 1))
 
-        @pl.when(i == pairs - 1)
-        def _():
-            @pl.when(pair == pairs - 1)
-            def _():
-                take_state()
-
+        @pl.when(i == pairs)
+        def _():
             finish_retention()
-
-        @pl.when(i == pairs)
-        def _():
             merge(block_at(i - 2))
 
         @pl.when(i == 1)

time: 188 us -> 177 us (0.941)
  Pallas kernels: 181 us -> 170 us
    pallas_call x1, Pallas kernels: 181 us -> 170 us  [body(): pl.pallas_call(functools.partial(kernel, sizes), out_shape=(jax.ShapeDtyp...]
where the time goes in v3:
time: 177 us
  Pallas kernels  170 us (96%)
  local copies, waits for them, and re-layouts  6.43 us (4%)
    pallas_call x1, Pallas kernels, body(): pl.pallas_call(functools.partial(kernel, sizes), out_shape=(jax.ShapeDtyp...  170 us
    unnamed x6, local copies, waits for them, and re-layouts  6.43 us

profile of v3, /device:TPU:0, one launch (start us, length us, event | category | flops | bytes accessed | tf_op | source)
XLA Modules:
  0.0 176.8 jit_solution(14255023528373824989)
XLA Ops:
  0.6 1.5 copy.20.ids
  2.2 1.5 copy.21.weights
  3.7 169.7 %fused.1 = (bf16[128,4096]{1,0:T(8,128)(2,1)}, bf16[512,1024]{1,0:T(8,128)(2,1)}) custom-call(bf16[4,128,4096]{2,1,0:T(8,128)(2,1)} %bitcast.3, f32[1,4096]{1,0:T(1,128)} %bitcast.4, s32[512,2]{1,0:T(8,128)} %copy.20.ids, f32[512,2]{1,0:T(8,128)} %copy.21.weights, bf16[1,4096,256]{2,1,0:T(8,128)(2,1)} %gate.1, bf16[1,4096,256]{2,1,0:T(8,128)(2,1)} %up.1, ...), custom_call_target="tpu_custom_call" | custom-call | tf_op jit(solution)/shard_map/fused/pallas_call | solution.py:736
  173.4 0.0 copy-start
  173.4 2.4 %copy.24 = bf16[128,4096]{1,0:T(8,128)(2,1)} copy(bf16[128,4096]{1,0:T(8,128)(2,1)} %get-tuple-element.4) | data formatting | bytes 2097152
  175.8 0.0 copy-done
  175.8 1.0 copy.25
Async XLA Ops:
  173.4 2.4 %copy-start = (bf16[512,1024]{1,0:T(8,128)(2,1)S(1)}, bf16[512,1024]{1,0:T(8,128)(2,1)}, u32[]{:S(2)}) copy-start(bf16[512,1024]{1,0:T(8,128)(2,1)} %get-tuple-element.5) | copy-start | bytes 3145732
